TPU v7x, 32 devices: a whole 2x2x4 slice. The times are simulated.
32 devices in a mesh: sp: 8 (over z, x), tp: 4 (over y, core).
Axes of the slice: x: 2, y: 2, z: 4, core: 2. Of those that a mesh axis runs over, the one named last changes fastest.
Arguments:
- queries: bfloat16 [512, 1024], P('tp', 'sp'), may hold values from -6 to 6
- input_key_matrix: bfloat16 [512, 1024], P('tp', 'sp'), may hold values from -6 to 6
- input_value_matrix: bfloat16 [1024, 1024], P('tp', 'sp'), may hold values from -6 to 6
- decay_preactivation: bfloat16 [512, 1024], P('tp', 'sp'), may hold values from -6 to 6
- extra_log_decay: float32 [512, 1024], P('tp', 'sp'), may hold values from -1 to 0, as said below
- channel_decay_speed: float32 [512], P('tp'), may hold values from 0 to 1, as said below
- output_weight_matrix: bfloat16 [2048, 1024], P(None, 'tp'), may hold values from -0.1875 to 0.1875
- stored_expert_rows: bfloat16 [1024, 2048], P('sp', 'tp'), may hold values from -6 to 6
- chosen_expert_index: int32 [1024, 2], P('sp'), may hold values from 0 to 7, all different within a row; in each aligned block of 128 rows (0 to 127, 128 to 255, ...) at most 48 rows name the same one
- expert_combine_weight: float32 [1024, 2], P('sp'), may hold values from 0.2 to 1
- cotangent: bfloat16 [1024, 2048], P('sp', 'tp'), may hold values from -6 to 6
- expert_gate_weight: bfloat16 [8, 2048, 2048], P('sp', None, 'tp'), may hold values from -0.125 to 0.125
- expert_up_weight: bfloat16 [8, 2048, 2048], P('sp', None, 'tp'), may hold values from -0.125 to 0.125
- expert_down_weight: bfloat16 [8, 2048, 2048], P('sp', 'tp'), may hold values from -0.125 to 0.125
Outputs:
- grad_queries: float32 [512, 1024], P('tp', 'sp')
- grad_keys: float32 [512, 1024], P('tp', 'sp')
- grad_values: float32 [1024, 1024], P('tp', 'sp')
- grad_logit: float32 [512, 1024], P('tp', 'sp')
- grad_out_proj: float32 [2048, 1024], P('sp', 'tp')
- grad_gate: bfloat16 [8, 2048, 2048], P('sp', None, 'tp')
- grad_up: bfloat16 [8, 2048, 2048], P('sp', None, 'tp')
- grad_down: bfloat16 [8, 2048, 2048], P('sp', 'tp')
Inputs may be any that keep to these rules, and one draw needn't show every extreme that they name: `chosen_expert_index`: each position names two different experts; in the rows of one device no expert is named more than 48 times. `channel_decay_speed`: positive. `extra_log_decay`: zero or negative.
All inputs are finite; a program needn't handle non-finite values.
Results may differ from a plain program's by a relative error of at most 0.023.
Values may be sent and summed in bfloat16 or wider, within the bound.
A program may use at most 64 MiB of HBM per device.

v0:
```python
import jax
import jax.numpy as jnp
from jax import lax
from jax.sharding import PartitionSpec as P

KEY_DIM = 32
VAL_DIM = 64


def prefix(shard, axis, combine, identity, reverse):
    peers, index = (lax.axis_size(axis), lax.axis_index(axis))
    everything = jax.tree.map(lambda part: lax.all_gather(part, axis), shard)
    start = jax.tree.map(
        lambda part, zero: jnp.broadcast_to(jnp.asarray(zero, part.dtype), part.shape),
        shard,
        identity,
    )

    def turn(k, before):
        at = peers - 1 - k if reverse else k
        reached = at > index if reverse else at < index
        new = combine(before, jax.tree.map(lambda part: part[at], everything))
        return jax.tree.map(lambda a, b: jnp.where(reached, a, b), new, before)

    return lax.fori_loop(0, peers, turn, start)


def combine(earlier, later):
    factor = earlier[0] * later[0]
    others = tuple(
        (
            later[0] * before_part + after_part
            for before_part, after_part in zip(earlier[1:], later[1:])
        )
    )
    return (factor,) + others


def summaries(key_feats, val_feats, decays):
    cumulative = jnp.cumsum(decays, axis=-1)
    total_log = cumulative[..., -1:]
    factor = jnp.exp(total_log)
    fwd_sum = jnp.einsum("hcs,hvs->hcv", key_feats * jnp.exp(total_log - cumulative), val_feats)
    bwd_sum = jnp.einsum("hcs,hvs->hcv", key_feats * jnp.exp(cumulative), val_feats)
    return (factor, fwd_sum, bwd_sum)


def mixing(scaled, key_feats, val_feats, decays, fwd_in, bwd_in):
    cumulative = jnp.cumsum(decays, axis=-1)
    total_log = cumulative[..., -1:]
    length = decays.shape[-1]
    lower_mask = lax.broadcasted_iota(jnp.int32, (length, length), 0) >= lax.broadcasted_iota(
        jnp.int32, (length, length), 1
    )
    log_gap = cumulative[..., :, None] - cumulative[..., None, :]
    weight = jnp.exp(jnp.where(lower_mask, log_gap, -log_gap))
    scores = jnp.einsum("hct,hcs,hcts->hts", scaled, key_feats, weight)
    inner_part = jnp.einsum("hts,hvs->hvt", scores, val_feats)
    carried = jnp.einsum("hct,hcv->hvt", scaled * jnp.exp(cumulative), fwd_in)
    carried = carried + jnp.einsum("hct,hcv->hvt", scaled * jnp.exp(total_log - cumulative), bwd_in)
    return inner_part + carried


def body(
    queries,
    input_key_matrix,
    input_value_matrix,
    decay_preactivation,
    extra_log_decay,
    channel_decay_speed,
    output_weight_matrix,
    stored_expert_rows,
    chosen_expert_index,
    expert_combine_weight,
    cotangent,
    expert_gate_weight,
    expert_up_weight,
    expert_down_weight,
):
    heads_here = input_value_matrix.shape[0] // VAL_DIM
    tok_rows = queries.shape[1]
    preactivation_single = decay_preactivation.astype(jnp.float32)
    decay_logarithm = (
        channel_decay_speed[:, None] * jax.nn.log_sigmoid(preactivation_single) + extra_log_decay
    )
    scaled = (queries.astype(jnp.float32) * KEY_DIM ** (-0.5)).reshape(
        heads_here, KEY_DIM, tok_rows
    )
    key_feats = input_key_matrix.astype(jnp.float32).reshape(heads_here, KEY_DIM, tok_rows)
    val_feats = input_value_matrix.astype(jnp.float32).reshape(heads_here, VAL_DIM, tok_rows)
    decays = decay_logarithm.reshape(heads_here, KEY_DIM, tok_rows)
    (factor, fwd_sum, bwd_sum), pull_sums = jax.vjp(summaries, key_feats, val_feats, decays)
    identity_pair = (jnp.ones_like(factor), jnp.zeros_like(fwd_sum))
    fwd_in = prefix((factor, fwd_sum), "sp", combine, identity_pair, False)[1]
    bwd_in = prefix((factor, bwd_sum), "sp", combine, identity_pair, True)[1]
    mixed, pull_mix = jax.vjp(mixing, scaled, key_feats, val_feats, decays, fwd_in, bwd_in)
    inv_rms = lax.rsqrt(jnp.mean(mixed * mixed, axis=1, keepdims=True) + 1e-06)
    normed = mixed * inv_rms
    mix_rows = normed.astype(jnp.bfloat16).reshape(-1, tok_rows)
    experts = lax.axis_size("sp")
    capacity = 3 * tok_rows // experts
    model_width = expert_gate_weight.shape[1]
    part_width = stored_expert_rows.shape[1]
    flat_ids = chosen_expert_index.reshape(-1)
    onehot = (flat_ids[:, None] == jnp.arange(experts, dtype=jnp.int32)[None, :]).astype(jnp.int32)
    slot_rank = jnp.sum((jnp.cumsum(onehot, axis=0) - onehot) * onehot, axis=1)
    slot_index = flat_ids * capacity + slot_rank
    slot_table = jnp.full((experts * capacity,), 2 * tok_rows, jnp.int32)
    slot_table = slot_table.at[slot_index].set(jnp.arange(2 * tok_rows, dtype=jnp.int32))
    weighted = (
        expert_combine_weight.reshape(-1, 1) * jnp.repeat(cotangent, 2, axis=0).astype(jnp.float32)
    ).astype(jnp.bfloat16)
    full_x, full_dy = (
        lax.all_gather(stored_expert_rows, "tp", axis=1, tiled=True),
        lax.all_gather(weighted, "tp", axis=1, tiled=True),
    )
    width_here = full_x.shape[1]
    zero_row = jnp.zeros((1, width_here), jnp.bfloat16)
    from_inputs = jnp.concatenate([full_x, zero_row], axis=0)[slot_table // 2]
    from_grads = jnp.concatenate([full_dy, zero_row], axis=0)[slot_table]
    send_x = from_inputs.reshape(experts, capacity, width_here)
    send_dy = from_grads.reshape(experts, capacity, width_here)
    recv_x, recv_dy = (
        lax.all_to_all(send_x, "sp", split_axis=0, concat_axis=0, tiled=True),
        lax.all_to_all(send_dy, "sp", split_axis=0, concat_axis=0, tiled=True),
    )
    rows_x = recv_x.reshape(-1, model_width)
    rows_dy = recv_dy.reshape(-1, model_width)
    gate_local = expert_gate_weight[0]
    up_local = expert_up_weight[0]
    down_local = expert_down_weight[0]
    contract_rows = (((0,), (0,)), ((), ()))
    contract_cols = (((1,), (1,)), ((), ()))
    gate_pre = jnp.dot(rows_x, gate_local, preferred_element_type=jnp.float32)
    up_pre = jnp.dot(rows_x, up_local, preferred_element_type=jnp.float32)
    gate_sig = jax.nn.sigmoid(gate_pre)
    gate_act = gate_pre * gate_sig
    hidden = (gate_act * up_pre).astype(jnp.bfloat16)
    grad_down = lax.dot_general(
        hidden, rows_dy, contract_rows, preferred_element_type=jnp.float32
    ).astype(jnp.bfloat16)
    grad_hidden = lax.dot_general(
        rows_dy, down_local, contract_cols, preferred_element_type=jnp.float32
    )
    grad_gate_pre = (grad_hidden * up_pre * gate_sig * (1.0 + gate_pre * (1.0 - gate_sig))).astype(
        jnp.bfloat16
    )
    grad_up_pre = (grad_hidden * gate_act).astype(jnp.bfloat16)
    grad_gate = lax.dot_general(
        rows_x, grad_gate_pre, contract_rows, preferred_element_type=jnp.float32
    ).astype(jnp.bfloat16)
    grad_up = lax.dot_general(
        rows_x, grad_up_pre, contract_rows, preferred_element_type=jnp.float32
    ).astype(jnp.bfloat16)
    partial_value = lax.dot_general(
        grad_gate_pre, gate_local, contract_cols, preferred_element_type=jnp.float32
    )
    partial_value = partial_value + lax.dot_general(
        grad_up_pre, up_local, contract_cols, preferred_element_type=jnp.float32
    )
    summed = lax.psum_scatter(
        partial_value.reshape(experts, capacity, model_width).astype(jnp.bfloat16),
        "tp",
        scatter_dimension=2,
        tiled=True,
    )
    returned_rows = lax.all_to_all(summed, "sp", split_axis=0, concat_axis=0, tiled=True).reshape(
        experts * capacity, part_width
    )
    picked = returned_rows[slot_index].astype(jnp.float32).reshape(tok_rows, 2, part_width)
    grad_rows = (cotangent.astype(jnp.float32) + picked[:, 0] + picked[:, 1]).astype(jnp.bfloat16)
    full_rows = lax.all_gather(grad_rows, "tp", axis=1, tiled=True)
    grad_out_proj = lax.psum_scatter(
        lax.dot_general(
            full_rows, mix_rows, (((0,), (1,)), ((), ())), preferred_element_type=jnp.float32
        ).astype(jnp.bfloat16),
        "sp",
        scatter_dimension=0,
        tiled=True,
    ).astype(jnp.float32)
    grad_normed = lax.dot_general(
        output_weight_matrix,
        full_rows,
        (((0,), (1,)), ((), ())),
        preferred_element_type=jnp.float32,
    )
    grad_normed = grad_normed.reshape(heads_here, VAL_DIM, tok_rows)
    grad_mixed = inv_rms * (
        grad_normed - normed * jnp.mean(grad_normed * normed, axis=1, keepdims=True)
    )
    cumulative = jnp.cumsum(decays, axis=-1)
    total_log = cumulative[..., -1:]
    fwd_source = jnp.einsum("hct,hvt->hcv", scaled * jnp.exp(cumulative), grad_mixed)
    bwd_source = jnp.einsum("hct,hvt->hcv", scaled * jnp.exp(total_log - cumulative), grad_mixed)
    grad_fwd_out = prefix((factor, fwd_source), "sp", combine, identity_pair, True)[1]
    grad_bwd_out = prefix((factor, bwd_source), "sp", combine, identity_pair, False)[1]
    grad_scaled, grad_keys_mix, grad_vals_mix, grad_decay_mix, unused_fwd, unused_bwd = pull_mix(
        grad_mixed
    )
    grad_factor = jnp.sum(grad_fwd_out * fwd_in + grad_bwd_out * bwd_in, axis=2, keepdims=True)
    grad_keys_sum, grad_vals_sum, grad_decay_sum = pull_sums(
        (grad_factor, grad_fwd_out, grad_bwd_out)
    )
    grad_queries = (grad_scaled * KEY_DIM ** (-0.5)).reshape(-1, tok_rows)
    grad_keys = (grad_keys_mix + grad_keys_sum).reshape(-1, tok_rows)
    grad_values = (grad_vals_mix + grad_vals_sum).reshape(-1, tok_rows)
    grad_decay = (grad_decay_mix + grad_decay_sum).reshape(-1, tok_rows)
    grad_logit = grad_decay * channel_decay_speed[:, None] * jax.nn.sigmoid(-preactivation_single)
    return (
        grad_queries,
        grad_keys,
        grad_values,
        grad_logit,
        grad_out_proj,
        grad_gate[None],
        grad_up[None],
        grad_down[None],
    )


def solution(mesh):
    in_specs = (
        P("tp", "sp"),
        P("tp", "sp"),
        P("tp", "sp"),
        P("tp", "sp"),
        P("tp", "sp"),
        P("tp"),
        P(None, "tp"),
        P("sp", "tp"),
        P("sp", None),
        P("sp", None),
        P("sp", "tp"),
        P("sp", None, "tp"),
        P("sp", None, "tp"),
        P("sp", "tp", None),
    )
    out_specs = (
        P("tp", "sp"),
        P("tp", "sp"),
        P("tp", "sp"),
        P("tp", "sp"),
        P("sp", "tp"),
        P("sp", None, "tp"),
        P("sp", None, "tp"),
        P("sp", "tp", None),
    )
    return jax.shard_map(body, mesh=mesh, in_specs=in_specs, out_specs=out_specs, check_vma=False)
```

profile of v0, /device:TPU:0, one launch (start us, length us, event | category | flops | bytes accessed | tf_op | source)
XLA Modules:
  0.0 367.7 jit_solution(17501311337254212600)
XLA Ops:
  12.9 8.9 %all_gather.52 = bf16[128,2048]{1,0:T(8,128)(2,1)S(1)} all-gather(bf16[128,512]{1,0:T(8,128)(2,1)} %param.29), channel_id=1, replica_groups=mesh['sp'=8,'tp'=4] {'tp'}, dimensions={1}, use_global_device_ids=true | all-gather | bytes 655360 | tf_op jit(solution)/shard_map/all_gather | solution.py:114
  21.8 3.1 gather_fusion.1
  24.9 5.9 %all-to-all-start.1 = ((bf16[8,48,2048]{2,1,0:T(8,128)(2,1)}), bf16[8,48,2048]{2,1,0:T(8,128)(2,1)}, u32[]{:S(2)}, u32[]{:S(2)}) async-start(bf16[8,48,2048]{2,1,0:T(8,128)(2,1)} %bitcast.197), calls=%async_computation.1 | async-start | bytes 3145728 | tf_op jit(solution)/shard_map/all_to_all | solution.py:124
  39.2 1.6 copy.159
  42.5 44.5 %all-gather = f32[32,32,1]{1,2,0:T(1,128)S(1)} all-gather(f32[4,32,1]{1,2,0:T(1,128)} %bitcast.224), channel_id=2, replica_groups=mesh['sp'=8,'tp'=4] {'sp'}, dimensions={0}, use_global_device_ids=true | all-gather | bytes 4608 | tf_op jit(solution)/shard_map/all_gather | solution.py:12
  90.3 33.6 %all-gather.2 = f32[32,32,64]{2,1,0:T(8,128)} all-gather(f32[4,32,64]{2,1,0:T(8,128)S(1)} %fusion.68), channel_id=4, replica_groups=mesh['sp'=8,'tp'=4] {'sp'}, dimensions={0}, use_global_device_ids=true | all-gather | bytes 294912 | tf_op jit(solution)/shard_map/all_gather | solution.py:12
  124.0 34.1 %all-gather.1 = f32[32,32,64]{2,1,0:T(8,128)} all-gather(f32[4,32,64]{2,1,0:T(8,128)S(1)} %fusion.67), channel_id=3, replica_groups=mesh['sp'=8,'tp'=4] {'sp'}, dimensions={0}, use_global_device_ids=true | all-gather | bytes 294912 | tf_op jit(solution)/shard_map/all_gather | solution.py:12
  159.5 3.2 gather_fusion
  162.7 4.4 %all-to-all-start = ((bf16[8,48,2048]{2,1,0:T(8,128)(2,1)}), bf16[8,48,2048]{2,1,0:T(8,128)(2,1)}, u32[]{:S(2)}, u32[]{:S(2)}) async-start(bf16[8,48,2048]{2,1,0:T(8,128)(2,1)} %bitcast.198), calls=%async_computation | async-start | bytes 3145728 | tf_op jit(solution)/shard_map/all_to_all | solution.py:125
  167.4 7.8 %while.61 = (s32[]{:T(128)}, f32[4,32,64]{2,1,0:T(8,128)S(1)}, s32[]{:T(128)}, f32[8,4,32,1]{2,1,3,0:T(4,128)S(1)}, f32[8,4,32,64]{3,2,1,0:T(8,128)}, /*index=5*/s32[]{:T(128)}, s32[]{:T(128)}) while((s32[]{:T(128)}, f32[4,32,64]{2,1,0:T(8,128)S(1)}, s32[]{:T(128)}, f32[8,4,32,1]{2,1,3,0:T(4,128)S(1)}, f32[8,4,32,64]{3,2,1,0:T(8,128)}, ...), condition=%wide.region_4.5_spmd.clone, body=%wide.region_3.4_spmd.clone.sunk | while | flops 32772 | bytes 99945 | solution.py:25
  175.5 2.5 fusion.28
  178.0 3.6 fusion.31
  181.6 7.6 %all-to-all-done = bf16[8,48,2048]{2,1,0:T(8,128)(2,1)} async-done(((bf16[8,48,2048]{2,1,0:T(8,128)(2,1)}), bf16[8,48,2048]{2,1,0:T(8,128)(2,1)}, u32[]{:S(2)}, u32[]{:S(2)}) %all-to-all-start) | async-done | bytes 1572896 | tf_op jit(solution)/shard_map/all_to_all | solution.py:125
  189.2 3.4 multiply_convert_fusion.1
  194.6 2.2 add_convert_fusion
  196.8 8.0 %while.60 = (s32[]{:T(128)}, f32[4,32,64]{2,1,0:T(8,128)S(1)}, s32[]{:T(128)}, f32[8,4,32,1]{2,1,3,0:T(4,128)S(1)}, f32[8,4,32,64]{3,2,1,0:T(8,128)}, /*index=5*/s32[]{:T(128)}, s32[]{:T(128)}, s32[]{:T(128)}, s32[]{:T(128)}) while((s32[]{:T(128)}, f32[4,32,64]{2,1,0:T(8,128)S(1)}, s32[]{:T(128)}, f32[8,4,32,1]{2,1,3,0:T(4,128)S(1)}, ...), condition=%wide.region_2.3_spmd.clone, body=%wide.region_1.2_spmd.clone.sunk | while | flops 32776 | bytes 100007 | solution.py:25
  205.0 5.1 %fusion.5 = bf16[4,128,128]{2,1,0:T(8,128)(2,1)S(1)} fusion(f32[4,32,128]{2,1,0:T(8,128)S(1)} %copy-done.32, f32[4,32,128]{2,1,0:T(8,128)S(1)} %bitcast.210, f32[4,32,128]{2,1,0:T(8,128)S(1)} %copy-done.15, pred[128,128]{1,0:T(8,128)(4,1)S(1)} %copy-done.39), kind=kLoop, calls=%fused_computation.20 | loop fusion | flops 12517376 | bytes 344064 | tf_op jit(solution)/shard_map/jvp(hct,hcs,hcts->hts)/dot_general | solution.py:57
  210.4 12.7 %reduce-scatter.3.cloned.1.call-done = bf16[8,48,512]{2,1,0:T(8,128)(2,1)} async-done(((bf16[8,48,2048]{2,1,0:T(8,128)(2,1)}), bf16[8,48,512]{2,1,0:T(8,128)(2,1)}) %reduce-scatter.3.cloned.1.call-update) | async-done | bytes 393232 | tf_op jit(solution)/shard_map/reduce_scatter | solution.py:161
  223.2 5.5 %all-to-all-start.2 = ((bf16[8,48,512]{2,1,0:T(8,128)(2,1)}), bf16[8,48,512]{2,1,0:T(8,128)(2,1)S(1)}, u32[]{:S(2)}, u32[]{:S(2)}) async-start(bf16[8,48,512]{2,1,0:T(8,128)(2,1)} %reduce-scatter.3.cloned.1.call-done), calls=%async_computation.3 | async-start | bytes 786432 | tf_op jit(solution)/shard_map/all_to_all | solution.py:167
  228.7 4.1 %fusion.23 = bf16[1,2048,512]{2,1,0:T(8,128)(2,1)} fusion(bf16[384,2048]{1,0:T(8,128)(2,1)} %bitcast.24, bf16[384,512]{1,0:T(8,128)(2,1)} %copy-done.21), kind=kOutput, calls=%fused_computation.41 | convolution fusion | flops 806354944 | bytes 4063232 | tf_op jit(solution)/shard_map/dot_general | solution.py:149
  232.9 4.2 %fusion.24 = bf16[1,2048,512]{2,1,0:T(8,128)(2,1)} fusion(bf16[384,2048]{1,0:T(8,128)(2,1)} %bitcast.24, bf16[384,512]{1,0:T(8,128)(2,1)S(1)} %copy-done.20), kind=kOutput, calls=%fused_computation.42 | convolution fusion | flops 806354944 | bytes 4063232 | tf_op jit(solution)/shard_map/dot_general | solution.py:152
  237.0 4.1 %fusion.25 = bf16[1,512,2048]{2,1,0:T(8,128)(2,1)} fusion(bf16[384,2048]{1,0:T(8,128)(2,1)} %bitcast.21, f32[384,512]{1,0:T(8,128)S(1)} %copy-done.48, f32[384,512]{1,0:T(8,128)S(1)} %copy-done.47), kind=kOutput, calls=%fused_computation.43 | convolution fusion | flops 807534592 | bytes 5242880 | tf_op jit(solution)/shard_map/dot_general | solution.py:139
  244.1 6.6 %all_gather.53 = bf16[128,2048]{1,0:T(8,128)(2,1)S(1)} all-gather(bf16[128,512]{1,0:T(8,128)(2,1)S(1)} %fusion.38), channel_id=1, replica_groups=mesh['sp'=8,'tp'=4] {'tp'}, dimensions={1}, use_global_device_ids=true | all-gather | bytes 655360 | tf_op jit(solution)/shard_map/all_gather | solution.py:172
  257.4 32.7 %all-gather.4 = f32[32,32,64]{2,1,0:T(8,128)S(1)} all-gather(f32[4,32,64]{2,1,0:T(8,128)S(1)} %fusion.75), channel_id=6, replica_groups=mesh['sp'=8,'tp'=4] {'sp'}, dimensions={0}, use_global_device_ids=true | all-gather | bytes 294912 | tf_op jit(solution)/shard_map/all_gather | solution.py:12
  292.2 31.8 %all-gather.3 = f32[32,32,64]{2,1,0:T(8,128)S(1)} all-gather(f32[4,32,64]{2,1,0:T(8,128)S(1)} %fusion.73), channel_id=5, replica_groups=mesh['sp'=8,'tp'=4] {'sp'}, dimensions={0}, use_global_device_ids=true | all-gather | bytes 294912 | tf_op jit(solution)/shard_map/all_gather | solution.py:12
  325.1 8.7 %fusion.14 = (f32[4,32,128]{2,1,0:T(8,128)S(1)}, f32[4,32,128]{2,1,0:T(8,128)S(1)}) fusion(f32[4,128,128]{2,1,0:T(8,128)} %fusion.72, f32[4,32,128]{2,1,0:T(8,128)} %copy.153, f32[4,32,128]{2,1,0:T(8,128)S(1)} %bitcast.211, f32[4,32,128]{2,1,0:T(8,128)S(1)} %copy-done.15, pred[128,128]{1,0:T(8,128)(4,1)S(1)} %copy-done.40), kind=kLoop, calls=%fused_computation.28 | loop fusion | flops 25133056 | bytes 606208 | tf_op jit(solution)/shard_map/transpose(jvp())/reduce_sum | solution.py:55
  336.5 2.9 fusion.9
  340.3 4.0 %fusion.11 = f32[4,32,1,128]{3,2,1,0:T(1,128)S(1)} fusion(f32[4,128,128]{2,1,0:T(8,128)} %fusion.72, f32[4,32,128]{2,1,0:T(8,128)S(1)} %copy-done.15, pred[128,128]{1,0:T(8,128)(4,1)S(1)} %copy-done.41, bf16[4,32,128,1]{2,1,0,3:T(8,128)(2,1)S(1)} %bitcast.222), kind=kOutput, calls=%fused_computation.26 | convolution fusion | flops 12582912 | bytes 442368 | tf_op jit(solution)/shard_map/transpose(jvp(hct,hcs,hcts->hts))/dot_general | solution.py:57
  346.5 3.0 pad_add_fusion
  354.9 1.7 copy.171
  356.6 1.7 copy.178
  359.5 1.6 convert_element_type.85
  (268 shorter events, 65.0 us)
Async XLA Ops:
  7.2 168.3 %copy-start = (bf16[1,2048,512]{2,1,0:T(8,128)(2,1)S(1)}, bf16[1,2048,512]{2,1,0:T(8,128)(2,1)}, u32[]{:S(2)}) copy-start(bf16[1,2048,512]{2,1,0:T(8,128)(2,1)} %param.33) | copy-start | bytes 6291460
  24.9 137.8 %all-to-all-start.1 = ((bf16[8,48,2048]{2,1,0:T(8,128)(2,1)}), bf16[8,48,2048]{2,1,0:T(8,128)(2,1)}, u32[]{:S(2)}, u32[]{:S(2)}) async-start(bf16[8,48,2048]{2,1,0:T(8,128)(2,1)} %bitcast.197), calls=%async_computation.1 | async-start | bytes 3145728 | tf_op jit(solution)/shard_map/all_to_all | solution.py:124
  30.9 127.3 %all-gather.7.cloned.1.call-start = ((), (), s32[]{:S(2)}) async-start(), calls=%async_computation.5 | async-start | bytes 1310720 | tf_op jit(solution)/shard_map/all_gather | solution.py:115
  32.8 57.3 %copy-start.9 = (bf16[256,128]{1,0:T(8,128)(2,1)S(1)}, bf16[256,128]{1,0:T(8,128)(2,1)}, u32[]{:S(2)}) copy-start(bf16[256,128]{1,0:T(8,128)(2,1)} %param.24) | copy-start | bytes 196612
  34.6 89.2 %copy-start.7 = (f32[4,32,128]{1,0,2:T(4,128)}, f32[4,32,128]{1,0,2:T(4,128)S(1)}, u32[]{:S(2)}) copy-start(f32[4,32,128]{1,0,2:T(4,128)S(1)} %copy.147) | copy-start | bytes 196612
  35.6 122.5 %copy-start.1 = (f32[4,32,128]{1,0,2:T(4,128)}, f32[4,32,128]{1,0,2:T(4,128)S(1)}, u32[]{:S(2)}) copy-start(f32[4,32,128]{1,0,2:T(4,128)S(1)} %copy.155) | copy-start | bytes 196612
  36.3 121.8 %copy-start.3 = (f32[4,32,128]{1,0,2:T(4,128)}, f32[4,32,128]{1,0,2:T(4,128)S(1)}, u32[]{:S(2)}) copy-start(f32[4,32,128]{1,0,2:T(4,128)S(1)} %copy.158) | copy-start | bytes 196612
  36.5 121.6 %copy-start.5 = (bf16[4,32,128]{1,0,2:T(4,128)(2,1)}, bf16[4,32,128]{1,0,2:T(4,128)(2,1)S(1)}, u32[]{:S(2)}) copy-start(bf16[4,32,128]{1,0,2:T(4,128)(2,1)S(1)} %copy.149) | copy-start | bytes 98308
  39.2 118.9 %copy-start.25 = (bf16[4,32,128]{2,1,0:T(8,128)(2,1)}, bf16[4,32,128]{2,1,0:T(8,128)(2,1)S(1)}, u32[]{:S(2)}) copy-start(bf16[4,32,128]{2,1,0:T(8,128)(2,1)S(1)} %copy.156) | copy-start | bytes 98308
  162.7 12.5 %copy-start.22 = (bf16[4,32,128]{2,1,0:T(8,128)(2,1)S(1)}, bf16[4,32,128]{2,1,0:T(8,128)(2,1)}, u32[]{:S(2)}) copy-start(bf16[4,32,128]{2,1,0:T(8,128)(2,1)} %copy.159) | copy-start | bytes 98308
  162.7 26.5 %all-to-all-start = ((bf16[8,48,2048]{2,1,0:T(8,128)(2,1)}), bf16[8,48,2048]{2,1,0:T(8,128)(2,1)}, u32[]{:S(2)}, u32[]{:S(2)}) async-start(bf16[8,48,2048]{2,1,0:T(8,128)(2,1)} %bitcast.198), calls=%async_computation | async-start | bytes 3145728 | tf_op jit(solution)/shard_map/all_to_all | solution.py:125
  167.2 56.0 %reduce-scatter.3.cloned.1.call-start = ((), (), s32[]{:S(2)}) async-start(), calls=%async_computation.6 | async-start | bytes 1966080 | tf_op jit(solution)/shard_map/reduce_scatter | solution.py:161
  178.0 11.2 %copy-start.46 = (f32[384,512]{1,0:T(8,128)}, f32[384,512]{1,0:T(8,128)S(1)}, u32[]{:S(2)}) copy-start(f32[384,512]{1,0:T(8,128)S(1)} %fusion.28) | copy-start | bytes 2359300
  196.7 8.1 %copy-start.27 = (bf16[4,32,128]{2,1,0:T(8,128)(2,1)S(1)}, bf16[4,32,128]{2,1,0:T(8,128)(2,1)}, u32[]{:S(2)}) copy-start(bf16[4,32,128]{2,1,0:T(8,128)(2,1)} %copy.161) | copy-start | bytes 98308
  196.7 8.3 %copy-start.15 = (f32[4,32,128]{2,1,0:T(8,128)S(1)}, f32[4,32,128]{2,1,0:T(8,128)}, u32[]{:S(2)}) copy-start(f32[4,32,128]{2,1,0:T(8,128)} %copy-done.14) | copy-start | bytes 196612
  196.7 8.3 %copy-start.29 = (f32[128,128]{1,0:T(8,128)S(1)}, f32[128,128]{1,0:T(8,128)}, u32[]{:S(2)}) copy-start(f32[128,128]{1,0:T(8,128)} %copy-done.28) | copy-start | bytes 196612
  196.7 8.3 %copy-start.32 = (f32[4,32,128]{2,1,0:T(8,128)S(1)}, f32[4,32,128]{2,1,0:T(8,128)}, u32[]{:S(2)}) copy-start(f32[4,32,128]{2,1,0:T(8,128)} %copy.153) | copy-start | bytes 196612
  196.7 8.3 %copy-start.39 = (pred[128,128]{1,0:T(8,128)(4,1)S(1)}, pred[128,128]{1,0:T(8,128)(4,1)}, u32[]{:S(2)}) copy-start(pred[128,128]{1,0:T(8,128)(4,1)} %iota_compare_fusion) | copy-start | bytes 49156
  210.2 22.6 %copy-start.16 = (bf16[4,128,128]{2,1,0:T(8,128)(2,1)}, bf16[4,128,128]{2,1,0:T(8,128)(2,1)S(1)}, u32[]{:S(2)}) copy-start(bf16[4,128,128]{2,1,0:T(8,128)(2,1)S(1)} %fusion.5) | copy-start | bytes 393220
  210.4 40.7 %copy-start.38 = (f32[4,128]{1,0:T(4,128)}, f32[4,128]{1,0:T(4,128)S(1)}, u32[]{:S(2)}) copy-start(f32[4,128]{1,0:T(4,128)S(1)} %add_rsqrt_fusion) | copy-start | bytes 6148
  223.2 17.9 %all-to-all-start.2 = ((bf16[8,48,512]{2,1,0:T(8,128)(2,1)}), bf16[8,48,512]{2,1,0:T(8,128)(2,1)S(1)}, u32[]{:S(2)}, u32[]{:S(2)}) async-start(bf16[8,48,512]{2,1,0:T(8,128)(2,1)} %reduce-scatter.3.cloned.1.call-done), calls=%async_computation.3 | async-start | bytes 786432 | tf_op jit(solution)/shard_map/all_to_all | solution.py:167
  228.6 130.9 %reduce-scatter.5.cloned.1.call-start = ((), (), s32[]{:S(2)}) async-start(), calls=%async_computation.7 | async-start | bytes 1179648 | tf_op jit(solution)/shard_map/reduce_scatter | solution.py:173
  242.7 8.0 %copy-start.13 = (bf16[2048,256]{1,0:T(8,128)(2,1)S(1)}, bf16[2048,256]{1,0:T(8,128)(2,1)}, u32[]{:S(2)}) copy-start(bf16[2048,256]{1,0:T(8,128)(2,1)} %param.28) | copy-start | bytes 3145732
  244.1 9.1 %copy-start.10 = (bf16[256,128]{1,0:T(8,128)(2,1)S(1)}, bf16[256,128]{1,0:T(8,128)(2,1)}, u32[]{:S(2)}) copy-start(bf16[256,128]{1,0:T(8,128)(2,1)} %param.24) | copy-start | bytes 196612
  257.4 67.7 %copy-start.30 = (f32[128,128]{1,0:T(8,128)S(1)}, f32[128,128]{1,0:T(8,128)}, u32[]{:S(2)}) copy-start(f32[128,128]{1,0:T(8,128)} %copy-done.28) | copy-start | bytes 196612
  257.4 67.8 %copy-start.40 = (pred[128,128]{1,0:T(8,128)(4,1)S(1)}, pred[128,128]{1,0:T(8,128)(4,1)}, u32[]{:S(2)}) copy-start(pred[128,128]{1,0:T(8,128)(4,1)} %iota_compare_fusion) | copy-start | bytes 49156
  325.1 11.4 %copy-start.31 = (f32[4,128,128]{2,1,0:T(8,128)S(1)}, f32[4,128,128]{2,1,0:T(8,128)}, u32[]{:S(2)}) copy-start(f32[4,128,128]{2,1,0:T(8,128)} %fusion.72) | copy-start | bytes 786436
  325.1 11.3 %copy-start.41 = (pred[128,128]{1,0:T(8,128)(4,1)S(1)}, pred[128,128]{1,0:T(8,128)(4,1)}, u32[]{:S(2)}) copy-start(pred[128,128]{1,0:T(8,128)(4,1)} %iota_compare_fusion) | copy-start | bytes 49156
  346.5 7.6 %copy-start.24 = (bf16[128,128]{0,1:T(8,128)(2,1)S(1)}, bf16[128,128]{0,1:T(8,128)(2,1)}, u32[]{:S(2)}) copy-start(bf16[128,128]{0,1:T(8,128)(2,1)} %copy-done.23) | copy-start | bytes 98308
  346.5 7.6 %copy-start.44 = (f32[128]{0:T(128)S(1)}, f32[128]{0:T(128)}, u32[]{:S(2)}) copy-start(f32[128]{0:T(128)} %param.27) | copy-start | bytes 1540
  349.5 9.0 %copy-start.26 = (bf16[4,32,128]{2,1,0:T(8,128)(2,1)S(1)}, bf16[4,32,128]{2,1,0:T(8,128)(2,1)}, u32[]{:S(2)}) copy-start(bf16[4,32,128]{2,1,0:T(8,128)(2,1)} %copy-done.25) | copy-start | bytes 98308
  349.5 9.2 %copy-start.17 = (bf16[4,128,128]{2,1,0:T(8,128)(2,1)S(1)}, bf16[4,128,128]{2,1,0:T(8,128)(2,1)}, u32[]{:S(2)}) copy-start(bf16[4,128,128]{2,1,0:T(8,128)(2,1)} %copy-done.16) | copy-start | bytes 393220
  (23 other events, 74.8 us)
Sparse Core Ops, SparseCore 0:
  33.8 17.6 all-gather.6
  196.9 26.2 reduce-scatter.2
  255.8 66.3 reduce-scatter.4
where the time goes:
time: 370 us; the launch traced here: 368 us
  blocking collectives  192 us (52%)
  other arithmetic  48.6 us (13%)
  matrix products  38.4 us (10%)
  local copies, waits for them, and re-layouts  36.1 us (10%)
  waiting for transfers between devices  20.4 us (6%)
  starting transfers between devices  16.2 us (4%)
  between operations  14.6 us (4%)
    all_gather x5, blocking collectives, prefix(): everything = jax.tree.map(lambda part: lax.all_gather(part, axis), shard)  177 us
    select_n x32, other arithmetic, turn(): return jax.tree.map(lambda a, b: jnp.where(reached, a, b), new, before)  16.6 us
    reduce_scatter x1, waiting for transfers between devices, body(): lax.psum_scatter(partial_value.reshape(experts, capacity, model_width).as...  12.7 us
    all_gather x1, blocking collectives, body(): lax.all_gather(stored_expert_rows, 'tp', axis=1, tiled=True)  8.87 us
    reduce_sum x1, other arithmetic, mixing(): log_gap = cumulative[..., :, None] - cumulative[..., None, :]  8.68 us
    all_to_all x1, waiting for transfers between devices, body(): lax.all_to_all(send_dy, 'sp', split_axis=0, concat_axis=0, tiled=True)  7.64 us
  transfers between devices with their start and end apart: 6, of which 2 were waited for; matrix products, arithmetic and copies ran while one was open for 26% of the time, Pallas kernels for 0%

commit v1 on v0

v1 whole, which is shorter than its diff:
```python
import functools

import jax
import jax.numpy as jnp
from jax import lax
from jax.experimental import pallas as pl
from jax.experimental.pallas import tpu as pltpu
from jax.sharding import PartitionSpec as P

KEY_DIM = 32
VAL_DIM = 64
BF16 = jnp.bfloat16
F32 = jnp.float32


def dot(a, b, contract):
    return lax.dot_general(a.astype(BF16), b.astype(BF16), (contract, ((), ())),
                           preferred_element_type=F32)


def exact_dot(a, b):
    return lax.dot_general(a, b, (((1,), (0,)), ((), ())), precision=lax.Precision.HIGHEST,
                           preferred_element_type=F32)


def triangle(length, test):
    rows = lax.broadcasted_iota(jnp.int32, (length, length), 0)
    cols = lax.broadcasted_iota(jnp.int32, (length, length), 1)
    return test(rows, cols)


def head_kernel(q_ref, k_ref, v_ref, pre_ref, extra_ref, speed_ref,
                st_ref, inner_ref, cum_ref, fwd_ref, bwd_ref):
    length = q_ref.shape[1]
    q = q_ref[...].astype(F32) * KEY_DIM ** (-0.5)
    k = k_ref[...].astype(F32)
    v = v_ref[...]
    pre = pre_ref[...].astype(F32)
    log_sig = jnp.minimum(pre, 0.0) - jnp.log1p(jnp.exp(-jnp.abs(pre)))
    decays = speed_ref[...] * log_sig + extra_ref[...]
    upto = triangle(length, lambda a, b: a <= b).astype(F32)
    cum = exact_dot(decays, upto)
    cum_ref[...] = cum
    cum_t = cum.T
    k_t = k.T
    total = jnp.zeros((length, length), F32)
    for c in range(KEY_DIM):
        weight = jnp.exp(-jnp.abs(cum_t[:, c:c + 1] - cum[c:c + 1, :]))
        total = total + (k_t[:, c:c + 1] * q[c:c + 1, :]) * weight
    scores = total.astype(BF16)
    st_ref[...] = scores
    inner_ref[...] = dot(v, scores, ((1,), (0,)))
    last = cum[:, length - 1:length]
    fwd = dot(k * jnp.exp(last - cum), v, ((1,), (1,)))
    bwd = dot(k * jnp.exp(cum), v, ((1,), (1,)))
    high = last.astype(BF16)
    rest = last - high.astype(F32)
    middle = rest.astype(BF16)
    low = (rest - middle.astype(F32)).astype(BF16)
    lane = lax.broadcasted_iota(jnp.int32, (KEY_DIM, VAL_DIM), 1)
    logs = jnp.where(lane == 0, high.astype(F32),
                     jnp.where(lane == 1, middle.astype(F32), low.astype(F32)))
    fwd_ref[...] = jnp.concatenate([fwd, logs], axis=1).astype(BF16)
    bwd_ref[...] = jnp.concatenate([bwd, logs], axis=1).astype(BF16)


def carry(recv, me, sums_of, factors):
    peers = recv.shape[0]
    zero = jnp.zeros((KEY_DIM, VAL_DIM), F32)
    before, after = zero, zero
    for i in range(peers):
        before = jnp.where(i < me, before * factors[i] + sums_of(i), before)
    for i in reversed(range(peers)):
        after = jnp.where(i > me, after * factors[i] + sums_of(i), after)
    return before, after


def factors_of(recv):
    out = []
    for i in range(recv.shape[0]):
        logs = recv[i, :, VAL_DIM:VAL_DIM + 3].astype(F32)
        out.append(jnp.exp(logs[:, 0:1] + logs[:, 1:2] + logs[:, 2:3]))
    return out


def mix_kernel(me_ref, recv_ref, q_ref, cum_ref, inner_ref,
               carried_ref, normed_ref, inv_ref, rows_ref):
    length = q_ref.shape[1]
    me = me_ref[0]
    fwd_in, bwd_in = carry(
        recv_ref, me, lambda i: recv_ref[i, :, :VAL_DIM].astype(F32), factors_of(recv_ref))
    carried_ref[...] = jnp.concatenate([fwd_in, bwd_in], axis=1)
    q = q_ref[...].astype(F32) * KEY_DIM ** (-0.5)
    cum = cum_ref[...]
    last = cum[:, length - 1:length]
    mixed = inner_ref[...] + dot(fwd_in, q * jnp.exp(cum), ((0,), (0,)))
    mixed = mixed + dot(bwd_in, q * jnp.exp(last - cum), ((0,), (0,)))
    inv = lax.rsqrt(jnp.mean(mixed * mixed, axis=0, keepdims=True) + 1e-06)
    normed = mixed * inv
    normed_ref[...] = normed
    inv_ref[...] = jnp.broadcast_to(inv, inv_ref.shape)
    rows_ref[...] = normed.astype(BF16)


def source_kernel(gn_ref, normed_ref, inv_ref, q_ref, cum_ref, dm_ref, fwd_ref, bwd_ref):
    length = q_ref.shape[1]
    normed = normed_ref[...]
    gn = gn_ref[...]
    dm = inv_ref[0:1, :] * (gn - normed * jnp.mean(gn * normed, axis=0, keepdims=True))
    dm_ref[...] = dm
    q = q_ref[...].astype(F32) * KEY_DIM ** (-0.5)
    cum = cum_ref[...]
    last = cum[:, length - 1:length]
    fwd = dot(q * jnp.exp(cum), dm, ((1,), (1,)))
    bwd = dot(q * jnp.exp(last - cum), dm, ((1,), (1,)))
    pad = jnp.zeros_like(fwd)
    fwd_ref[...] = jnp.concatenate([fwd, pad], axis=1).astype(BF16)
    bwd_ref[...] = jnp.concatenate([bwd, pad], axis=1).astype(BF16)


def inner_kernel(dm_ref, q_ref, k_ref, v_ref, cum_ref, st_ref, carried_ref,
                 dq_ref, dk_ref, dv_ref, dc_ref, dt_ref):
    length = q_ref.shape[1]
    dm = dm_ref[...]
    q = q_ref[...].astype(F32) * KEY_DIM ** (-0.5)
    k = k_ref[...].astype(F32)
    v = v_ref[...]
    cum = cum_ref[...]
    by_query = dot(dm, v, ((0,), (0,)))
    by_key = dot(v, dm, ((0,), (0,)))
    sign = jnp.where(triangle(length, lambda a, b: a > b), 1.0,
                     jnp.where(triangle(length, lambda a, b: a < b), -1.0, 0.0)).astype(F32)
    by_query_signed = by_query * sign
    by_key_signed = by_key * -sign
    cum_t, q_t, k_t = cum.T, q.T, k.T
    dq, dk, dq_signed, dk_signed = [], [], [], []
    for c in range(KEY_DIM):
        weight = jnp.exp(-jnp.abs(cum_t[:, c:c + 1] - cum[c:c + 1, :]))
        with_q = weight * q_t[:, c:c + 1]
        with_k = weight * k_t[:, c:c + 1]
        dk.append(jnp.sum(by_query * with_q, axis=0, keepdims=True))
        dk_signed.append(jnp.sum(by_query_signed * with_q, axis=0, keepdims=True))
        dq.append(jnp.sum(by_key * with_k, axis=0, keepdims=True))
        dq_signed.append(jnp.sum(by_key_signed * with_k, axis=0, keepdims=True))
    join = lambda rows: jnp.concatenate(rows, axis=0)
    last = cum[:, length - 1:length]
    carried = carried_ref[...]
    up, down = jnp.exp(cum), jnp.exp(last - cum)
    d_up = dot(carried[:, :VAL_DIM], dm, ((1,), (0,))) * up
    d_down = dot(carried[:, VAL_DIM:], dm, ((1,), (0,))) * down
    dq_ref[...] = (join(dq) + d_up + d_down) * KEY_DIM ** (-0.5)
    dk_ref[...] = join(dk)
    dv_ref[...] = dot(dm, st_ref[...], ((1,), (1,)))
    dc_ref[...] = q * (join(dq_signed) + d_up - d_down) - k * join(dk_signed)
    dt_ref[...] = jnp.broadcast_to(
        jnp.sum(q * d_down, axis=1, keepdims=True), dt_ref.shape)


def last_kernel(me_ref, recv_ref, first_ref, carried_ref, k_ref, v_ref, cum_ref,
                pre_ref, speed_ref, dk_in_ref, dv_in_ref, dc_in_ref, dt_ref,
                dk_ref, dv_ref, logit_ref):
    length = k_ref.shape[1]
    me = me_ref[0]
    grad_bwd, grad_fwd = carry(
        recv_ref, me, lambda i: recv_ref[i, :, :VAL_DIM].astype(F32), factors_of(first_ref))
    k = k_ref[...].astype(F32)
    v = v_ref[...]
    cum = cum_ref[...]
    last = cum[:, length - 1:length]
    up, down = jnp.exp(cum), jnp.exp(last - cum)
    d_down = dot(grad_fwd, v, ((1,), (0,))) * down
    d_up = dot(grad_bwd, v, ((1,), (0,))) * up
    dk_ref[...] = dk_in_ref[...] + d_down + d_up
    dv_ref[...] = (dv_in_ref[...] + dot(grad_fwd, k * down, ((0,), (0,)))
                   + dot(grad_bwd, k * up, ((0,), (0,))))
    carried = carried_ref[...]
    grad_factor = jnp.sum(grad_fwd * carried[:, :VAL_DIM] + grad_bwd * carried[:, VAL_DIM:],
                          axis=1, keepdims=True)
    grad_total = (dt_ref[:, 0:1] + jnp.sum(k * d_down, axis=1, keepdims=True)
                  + grad_factor * jnp.exp(last))
    dc = dc_in_ref[...] + k * (d_up - d_down)
    from_here = triangle(length, lambda a, b: a >= b).astype(F32)
    grad_decay = exact_dot(dc, from_here) + grad_total
    pre = pre_ref[...].astype(F32)
    logit_ref[...] = grad_decay * speed_ref[...] * jax.nn.sigmoid(-pre)


def per_head(kernel, heads, outs, args, vmem_ops, scalars=0):
    def spec(shape):
        if len(shape) == 3:
            return pl.BlockSpec((shape[0], shape[1] // heads, shape[2]), lambda h: (0, h, 0))
        return pl.BlockSpec((shape[0] // heads, shape[1]), lambda h: (h, 0))

    in_specs = [pl.BlockSpec(memory_space=pltpu.SMEM)] * scalars
    in_specs += [spec(arg.shape) for arg in args[scalars:]]
    return pl.pallas_call(
        kernel,
        grid=(heads,),
        in_specs=in_specs,
        out_specs=[spec(shape) for shape, _ in outs],
        out_shape=[jax.ShapeDtypeStruct(shape, dtype) for shape, dtype in outs],
        cost_estimate=pl.CostEstimate(
            flops=vmem_ops * heads, bytes_accessed=1 << 20, transcendentals=0),
        compiler_params=pltpu.CompilerParams(dimension_semantics=("arbitrary",)),
    )(*args)


def body(
    queries,
    input_key_matrix,
    input_value_matrix,
    decay_preactivation,
    extra_log_decay,
    channel_decay_speed,
    output_weight_matrix,
    stored_expert_rows,
    chosen_expert_index,
    expert_combine_weight,
    cotangent,
    expert_gate_weight,
    expert_up_weight,
    expert_down_weight,
):
    heads = input_value_matrix.shape[0] // VAL_DIM
    tok_rows = queries.shape[1]
    experts = lax.axis_size("sp")
    index = lax.axis_index("sp")
    me = index.astype(jnp.int32).reshape(1)
    capacity = 3 * tok_rows // experts
    slots = experts * capacity
    part_width = stored_expert_rows.shape[1]
    model_width = expert_gate_weight.shape[1]
    channels = heads * KEY_DIM
    values = heads * VAL_DIM
    tn = (((0,), (0,)), ((), ()))
    nt = (((1,), (1,)), ((), ()))

    expert_ids = lax.broadcasted_iota(jnp.int32, (tok_rows, experts), 1)
    picks = [chosen_expert_index[:, i:i + 1] == expert_ids for i in range(2)]
    earlier = triangle(tok_rows, lambda a, b: a > b).astype(BF16)
    counts = jnp.dot(earlier, (picks[0] | picks[1]).astype(BF16), preferred_element_type=F32)
    slot_ids = lax.broadcasted_iota(jnp.int32, (tok_rows, slots), 1)
    places = []
    for i in range(2):
        rank = jnp.sum(jnp.where(picks[i], counts, 0.0), axis=1, keepdims=True)
        slot = chosen_expert_index[:, i:i + 1] * capacity + rank.astype(jnp.int32)
        places.append((slot == slot_ids).astype(BF16))
    place = places[0] + places[1]
    weighted = [
        (expert_combine_weight[:, i:i + 1] * cotangent.astype(F32)).astype(BF16)
        for i in range(2)
    ]
    send_x = lax.dot_general(place, stored_expert_rows, tn, preferred_element_type=F32)
    send_dy = lax.dot_general(jnp.concatenate(places, axis=0), jnp.concatenate(weighted, axis=0),
                              tn, preferred_element_type=F32)

    def exchange(rows):
        rows = rows.astype(BF16).reshape(experts, capacity, part_width)
        rows = lax.all_to_all(rows, "sp", split_axis=0, concat_axis=0, tiled=True)
        return lax.all_gather(rows.reshape(slots, part_width), "tp", axis=1, tiled=True)

    rows_x = exchange(send_x)
    rows_dy = exchange(send_dy)

    speed = channel_decay_speed[:, None]
    state = ((channels, 2 * VAL_DIM), BF16)
    scores, inner, cum, fwd_sum, bwd_sum = per_head(
        head_kernel, heads,
        [((heads * tok_rows, tok_rows), BF16), ((values, tok_rows), F32),
         ((channels, tok_rows), F32), state, state],
        [queries, input_key_matrix, input_value_matrix, decay_preactivation, extra_log_decay,
         speed], 1 << 28)
    peer = lax.broadcasted_iota(jnp.int32, (experts, 1, 1), 0)
    sums = lax.all_to_all(jnp.where(peer > index, fwd_sum[None], bwd_sum[None]),
                          "sp", split_axis=0, concat_axis=0, tiled=True)
    carried, normed, inv_rms, mix_rows = per_head(
        mix_kernel, heads,
        [((channels, 2 * VAL_DIM), F32), ((values, tok_rows), F32), ((heads * 8, tok_rows), F32),
         ((values, tok_rows), BF16)],
        [me, sums, queries, cum, inner], 1 << 26, scalars=1)

    gate_local = expert_gate_weight[0]
    up_local = expert_up_weight[0]
    down_local = expert_down_weight[0]
    gate_pre = jnp.dot(rows_x, gate_local, preferred_element_type=F32)
    up_pre = jnp.dot(rows_x, up_local, preferred_element_type=F32)
    gate_sig = jax.nn.sigmoid(gate_pre)
    gate_act = gate_pre * gate_sig
    hidden = (gate_act * up_pre).astype(BF16)
    grad_hidden = lax.dot_general(rows_dy, down_local, nt, preferred_element_type=F32)
    grad_gate_pre = (grad_hidden * up_pre * gate_sig * (1.0 + gate_pre * (1.0 - gate_sig))).astype(
        BF16
    )
    grad_up_pre = (grad_hidden * gate_act).astype(BF16)
    partial_value = lax.dot_general(grad_gate_pre, gate_local, nt, preferred_element_type=F32)
    partial_value = partial_value + lax.dot_general(
        grad_up_pre, up_local, nt, preferred_element_type=F32
    )
    summed = lax.psum_scatter(
        partial_value.astype(BF16), "tp", scatter_dimension=1, tiled=True
    ).reshape(experts, capacity, part_width)
    grad_down = lax.dot_general(hidden, rows_dy, tn, preferred_element_type=F32).astype(BF16)
    grad_gate = lax.dot_general(rows_x, grad_gate_pre, tn, preferred_element_type=F32).astype(BF16)
    grad_up = lax.dot_general(rows_x, grad_up_pre, tn, preferred_element_type=F32).astype(BF16)
    returned = lax.all_to_all(summed, "sp", split_axis=0, concat_axis=0, tiled=True)
    picked = jnp.dot(place, returned.reshape(slots, part_width), preferred_element_type=F32)
    grad_rows = (cotangent.astype(F32) + picked).astype(BF16)
    full_rows = lax.all_gather(grad_rows, "tp", axis=1, tiled=True)
    grad_normed = lax.dot_general(
        output_weight_matrix, full_rows, (((0,), (1,)), ((), ())), preferred_element_type=F32
    )
    grad_out_proj = lax.psum_scatter(
        lax.dot_general(
            full_rows, mix_rows, (((0,), (1,)), ((), ())), preferred_element_type=F32
        ).astype(BF16),
        "sp",
        scatter_dimension=0,
        tiled=True,
    ).astype(F32)
    grad_mixed, fwd_source, bwd_source = per_head(
        source_kernel, heads, [((values, tok_rows), F32), state, state],
        [grad_normed, normed, inv_rms, queries, cum], 1 << 26)
    sources = lax.all_to_all(jnp.where(peer < index, fwd_source[None], bwd_source[None]),
                             "sp", split_axis=0, concat_axis=0, tiled=True)
    by_channel = ((channels, tok_rows), F32)
    grad_queries, dk, dv, dc, dt = per_head(
        inner_kernel, heads,
        [by_channel, by_channel, ((values, tok_rows), F32), by_channel, by_channel],
        [grad_mixed, queries, input_key_matrix, input_value_matrix, cum, scores, carried],
        1 << 29)
    grad_keys, grad_values, grad_logit = per_head(
        last_kernel, heads, [by_channel, ((values, tok_rows), F32), by_channel],
        [me, sources, sums, carried, input_key_matrix, input_value_matrix, cum,
         decay_preactivation, speed, dk, dv, dc, dt], 1 << 26, scalars=1)
    return (
        grad_queries,
        grad_keys,
        grad_values,
        grad_logit,
        grad_out_proj,
        grad_gate[None],
        grad_up[None],
        grad_down[None],
    )


def solution(mesh):
    in_specs = (
        P("tp", "sp"),
        P("tp", "sp"),
        P("tp", "sp"),
        P("tp", "sp"),
        P("tp", "sp"),
        P("tp"),
        P(None, "tp"),
        P("sp", "tp"),
        P("sp", None),
        P("sp", None),
        P("sp", "tp"),
        P("sp", None, "tp"),
        P("sp", None, "tp"),
        P("sp", "tp", None),
    )
    out_specs = (
        P("tp", "sp"),
        P("tp", "sp"),
        P("tp", "sp"),
        P("tp", "sp"),
        P("sp", "tp"),
        P("sp", None, "tp"),
        P("sp", None, "tp"),
        P("sp", "tp", None),
    )
    return jax.shard_map(body, mesh=mesh, in_specs=in_specs, out_specs=out_specs, check_vma=False)
```

time: 370 us -> 205 us (0.55)
  blocking collectives: 192 us -> 55.5 us
  other arithmetic: 48.6 us -> 5.99 us
  waiting for transfers between devices: 20.4 us -> 59.9 us
  local copies, waits for them, and re-layouts: 36.1 us -> 3.65 us
  Pallas kernels: 0 us -> 26.9 us
  matrix products: 38.4 us -> 28.5 us
  starting transfers between devices: 16.2 us -> 9.36 us
    all_gather x6 -> x0, blocking collectives: 186 us -> none  [the longest x5 177 us: prefix(): everything = jax.tree.map(lambda part: lax.all_gather(part, axis), shard)]
    all_to_all x0 -> x3, blocking collectives: none -> 49 us  [the longest x2 34.3 us: exchange(): rows = lax.all_to_all(rows, 'sp', split_axis=0, concat_axis=0, tiled=True)]
    reduce_scatter x1, waiting for transfers between devices: 0.01 us -> 30.6 us  [body(): lax.psum_scatter(lax.dot_general(full_rows, mix_rows, (((0,), (1,)), ((),...]
    pallas_call x0 -> x5, Pallas kernels: none -> 26.9 us  [per_head(): pl.pallas_call(kernel, grid=(heads,), in_specs=in_specs, out_specs=[spec(...]
    all_gather x1 -> x2, waiting for transfers between devices: 0.02 us -> 17.1 us  [exchange(): lax.all_gather(rows.reshape(slots, part_width), 'tp', axis=1, tiled=True)]
    select_n x34 -> x2, other arithmetic: 17.2 us -> 2.47 us  [the longest x1 1.57 us: body(): jnp.where(peer < index, fwd_source[None], bwd_source[None])]
    dot_general x25 -> x12, matrix products: 36.6 us -> 25 us  [the longest x1 4.17 us: body(): lax.dot_general(rows_x, grad_gate_pre, tn, preferred_element_type=F32)]
    reduce_sum x4 -> x0, other arithmetic: 10.1 us -> none  [the longest x1 8.68 us: mixing(): log_gap = cumulative[..., :, None] - cumulative[..., None, :]]
  transfers between devices with their start and end apart: 6 -> 6, of which waited for: 2 -> 5; matrix products, arithmetic and copies ran while one was open for 26% -> 11% of each run, Pallas kernels for 0% -> 13%
where the time goes in v1:
time: 205 us; the launch traced here: 204 us
  waiting for transfers between devices  59.9 us (29%)
  blocking collectives  55.5 us (27%)
  matrix products  28.5 us (14%)
  Pallas kernels  26.9 us (13%)
  between operations  13.9 us (7%)
  starting transfers between devices  9.36 us (5%)
  other arithmetic  5.99 us (3%)
  local copies, waits for them, and re-layouts  3.65 us (2%)
    all_to_all x2, blocking collectives, exchange(): rows = lax.all_to_all(rows, 'sp', split_axis=0, concat_axis=0, tiled=True)  34.3 us
    reduce_scatter x1, waiting for transfers between devices, body(): lax.psum_scatter(lax.dot_general(full_rows, mix_rows, (((0,), (1,)), ((),...  30.6 us
    pallas_call x5, Pallas kernels, per_head(): pl.pallas_call(kernel, grid=(heads,), in_specs=in_specs, out_specs=[spec(...  26.9 us
    all_gather x2, waiting for transfers between devices, exchange(): lax.all_gather(rows.reshape(slots, part_width), 'tp', axis=1, tiled=True)  17.1 us
    all_to_all x1, blocking collectives, body(): lax.all_to_all(jnp.where(peer > index, fwd_sum[None], bwd_sum[None]), 'sp...  14.7 us
    all_to_all x1, waiting for transfers between devices, body(): lax.all_to_all(summed, 'sp', split_axis=0, concat_axis=0, tiled=True)  7.75 us
    all_gather x1, blocking collectives, body(): full_rows = lax.all_gather(grad_rows, 'tp', axis=1, tiled=True)  6.5 us
    all_to_all x1, starting transfers between devices, body(): lax.all_to_all(summed, 'sp', split_axis=0, concat_axis=0, tiled=True)  5.51 us
  transfers between devices with their start and end apart: 6, of which 5 were waited for; matrix products, arithmetic and copies ran while one was open for 11% of the time, Pallas kernels for 13%

profile of v1, /device:TPU:0, one launch (start us, length us, event | category | flops | bytes accessed | tf_op | source)
XLA Modules:
  0.0 203.8 jit_solution(11992884412768420962)
XLA Ops:
  7.2 0.8 slice_bitcast_fusion.3
  9.0 1.3 convolution_convert_fusion.4
  10.3 19.2 %all_to_all.25 = bf16[8,48,512]{2,1,0:T(8,128)(2,1)} all-to-all(bf16[8,48,512]{2,1,0:T(8,128)(2,1)S(1)} %bitcast.69), channel_id=1, replica_groups=mesh['sp'=8,'tp'=4] {'sp'}, dimensions={0} | all-to-all | bytes 786432 | tf_op jit(solution)/shard_map/all_to_all | solution.py:259
  30.4 1.0 fusion.14
  31.8 15.1 %all_to_all.26 = bf16[8,48,512]{2,1,0:T(8,128)(2,1)} all-to-all(bf16[8,48,512]{2,1,0:T(8,128)(2,1)S(1)} %bitcast.72), channel_id=1, replica_groups=mesh['sp'=8,'tp'=4] {'sp'}, dimensions={0} | all-to-all | bytes 786432 | tf_op jit(solution)/shard_map/all_to_all | solution.py:259
  46.9 1.1 all-gather.5.cloned.1.call-done
  48.1 3.4 %fusion.5 = f32[384,512]{1,0:T(8,128)} fusion(bf16[384,2048]{1,0:T(8,128)(2,1)} %all-gather.5.cloned.1.call-done, bf16[1,2048,512]{2,1,0:T(8,128)(2,1)S(1)} %copy-done), kind=kOutput, calls=%fused_computation.10 | convolution fusion | flops 805306368 | bytes 4456448 | tf_op jit(solution)/shard_map/dot_general | solution.py:285
  51.5 1.9 fusion.8
  53.3 15.9 %all-gather.3.cloned.1.call-done = bf16[384,2048]{1,0:T(8,128)(2,1)} async-done(((bf16[384,512]{1,0:T(8,128)(2,1)}), bf16[384,2048]{1,0:T(8,128)(2,1)}) %all-gather.3.cloned.1.call-update) | async-done | bytes 1572880 | tf_op jit(solution)/shard_map/all_gather | solution.py:260
  69.3 3.7 %multiply_convert_fusion.1 = (bf16[384,512]{1,0:T(8,128)(2,1)S(1)}, bf16[384,512]{1,0:T(8,128)(2,1)S(1)}) fusion(f32[384,512]{1,0:T(8,128)} %fusion.5, f32[384,512]{1,0:T(8,128)} %fusion.8, bf16[384,2048]{1,0:T(8,128)(2,1)} %all-gather.3.cloned.1.call-done, bf16[1,512,2048]{2,1,0:T(8,128)(2,1)} %param.27), kind=kOutput, calls=%fused_computation.23 | convolution fusion | flops 807862272 | bytes 6029312 | tf_op jit(solution)/shard_map/dot_general | solution.py:290
  73.0 1.0 fusion.3
  74.5 2.2 %add_convert_fusion = bf16[384,2048]{1,0:T(8,128)(2,1)} fusion(f32[384,2048]{1,0:T(8,128)S(1)} %fusion.3, bf16[384,512]{1,0:T(8,128)(2,1)S(1)} %get-tuple-element.50, bf16[1,2048,512]{2,1,0:T(8,128)(2,1)S(1)} %copy-done.2), kind=kOutput, calls=%fused_computation | convolution fusion | flops 806879232 | bytes 7208960 | tf_op jit(solution)/shard_map/dot_general | solution.py:296
  77.5 7.4 %shard_map.197 = (bf16[512,128]{1,0:T(8,128)(2,1)}, f32[256,128]{1,0:T(8,128)}, f32[128,128]{1,0:T(8,128)}, bf16[128,128]{1,0:T(8,128)(2,1)}, bf16[128,128]{1,0:T(8,128)(2,1)}) custom-call(bf16[128,128]{1,0:T(8,128)(2,1)} %q_ref.7, bf16[128,128]{1,0:T(8,128)(2,1)} %k_ref.5, bf16[256,128]{1,0:T(8,128)(2,1)} %v_ref.5, bf16[128,128]{1,0:T(8,128)(2,1)} %pre_ref.3, ...), custom_call_target="tpu_custom_call" | custom-call | flops 1073741824 | bytes 1048576 | tf_op jit(solution)/shard_map/pallas_call | solution.py:196
  84.9 0.9 broadcast_select_fusion.1
  85.8 14.7 %all_to_all.27.recv_ref.first_ref = bf16[8,128,128]{2,1,0:T(8,128)(2,1)} all-to-all(bf16[8,128,128]{2,1,0:T(8,128)(2,1)S(1)} %broadcast_select_fusion.1), channel_id=1, replica_groups=mesh['sp'=8,'tp'=4] {'sp'}, dimensions={0} | all-to-all | bytes 524288 | tf_op jit(solution)/shard_map/all_to_all | solution.py:274
  100.6 4.4 %reduce-scatter.3.cloned.1.call-done = bf16[384,512]{1,0:T(8,128)(2,1)} async-done(((bf16[384,2048]{1,0:T(8,128)(2,1)}), bf16[384,512]{1,0:T(8,128)(2,1)}) %reduce-scatter.3.cloned.1.call-update) | async-done | bytes 393232 | tf_op jit(solution)/shard_map/reduce_scatter | solution.py:299
  105.0 5.5 %all-to-all-start.2 = ((bf16[8,48,512]{2,1,0:T(8,128)(2,1)}), bf16[8,48,512]{2,1,0:T(8,128)(2,1)S(1)}, u32[]{:S(2)}, u32[]{:S(2)}) async-start(bf16[8,48,512]{2,1,0:T(8,128)(2,1)} %bitcast.70), calls=%async_computation.3 | async-start | bytes 786432 | tf_op jit(solution)/shard_map/all_to_all | solution.py:305
  110.6 3.8 %shard_map.198 = (f32[128,128]{1,0:T(8,128)}, f32[256,128]{1,0:T(8,128)}, f32[32,128]{1,0:T(8,128)}, bf16[256,128]{1,0:T(8,128)(2,1)}) custom-call(s32[1]{0:T(128)} %bitcast.18.me_ref, bf16[8,128,128]{2,1,0:T(8,128)(2,1)} %all_to_all.27.recv_ref.first_ref, bf16[128,128]{1,0:T(8,128)(2,1)} %q_ref.7, f32[128,128]{1,0:T(8,128)} %get-tuple-element.30.cum_ref, ...), custom_call_target="tpu_custom_call" | custom-call | flops 268435456 | bytes 1048576 | tf_op jit(solution)/shard_map/pallas_call | solution.py:196
  114.3 7.7 %all-to-all-done.2 = bf16[8,48,512]{2,1,0:T(8,128)(2,1)S(1)} async-done(((bf16[8,48,512]{2,1,0:T(8,128)(2,1)}), bf16[8,48,512]{2,1,0:T(8,128)(2,1)S(1)}, u32[]{:S(2)}, u32[]{:S(2)}) %all-to-all-start.2) | async-done | bytes 393248 | tf_op jit(solution)/shard_map/all_to_all | solution.py:305
  122.4 6.5 %all_gather.11 = bf16[128,2048]{1,0:T(8,128)(2,1)S(1)} all-gather(bf16[128,512]{1,0:T(8,128)(2,1)S(1)} %fusion.12), channel_id=1, replica_groups=mesh['sp'=8,'tp'=4] {'tp'}, dimensions={1}, use_global_device_ids=true | all-gather | bytes 655360 | tf_op jit(solution)/shard_map/all_gather | solution.py:308
  128.9 2.3 %convolution_convert_fusion.3 = bf16[2048,256]{1,0:T(8,128)(2,1)} fusion(bf16[128,2048]{1,0:T(8,128)(2,1)S(1)} %all_gather.11, bf16[256,128]{1,0:T(8,128)(2,1)} %get-tuple-element.47), kind=kOutput, calls=%fused_computation.7 | convolution fusion | flops 134742016 | bytes 1638400 | tf_op jit(solution)/shard_map/dot_general | solution.py:313
  131.2 4.2 %fusion = bf16[1,2048,512]{2,1,0:T(8,128)(2,1)} fusion(bf16[384,2048]{1,0:T(8,128)(2,1)} %all-gather.5.cloned.1.call-done, bf16[384,512]{1,0:T(8,128)(2,1)S(1)} %get-tuple-element.51), kind=kOutput, calls=%fused_computation.4 | convolution fusion | flops 806354944 | bytes 4063232 | tf_op jit(solution)/shard_map/dot_general | solution.py:303
  135.4 2.7 %fusion.2 = bf16[1,512,2048]{2,1,0:T(8,128)(2,1)} fusion(bf16[384,2048]{1,0:T(8,128)(2,1)S(1)} %copy-done.8, f32[384,512]{1,0:T(8,128)S(1)} %copy-done.10, f32[384,512]{1,0:T(8,128)S(1)} %copy-done.9), kind=kOutput, calls=%fused_computation.6 | convolution fusion | flops 807534592 | bytes 5242880 | tf_op jit(solution)/shard_map/dot_general | solution.py:302
  138.1 1.2 convolution_bitcast_fusion.gn_ref
  139.2 3.2 %shard_map.199 = (f32[256,128]{1,0:T(8,128)}, bf16[128,128]{1,0:T(8,128)(2,1)}, bf16[128,128]{1,0:T(8,128)(2,1)}) custom-call(f32[256,128]{1,0:T(8,128)} %convolution_bitcast_fusion.gn_ref, f32[256,128]{1,0:T(8,128)} %get-tuple-element.32.normed_ref, f32[32,128]{1,0:T(8,128)} %get-tuple-element.33.inv_ref, bf16[128,128]{1,0:T(8,128)(2,1)} %q_ref.7, ...), custom_call_target="tpu_custom_call" | custom-call | flops 268435456 | bytes 1048576 | tf_op jit(solution)/shard_map/pallas_call | solution.py:196
  142.4 1.6 broadcast_select_fusion
  144.0 3.7 %all-to-all-start.4 = ((bf16[8,128,128]{2,1,0:T(8,128)(2,1)}), bf16[8,128,128]{2,1,0:T(8,128)(2,1)S(1)}, u32[]{:S(2)}, u32[]{:S(2)}) async-start(bf16[8,128,128]{2,1,0:T(8,128)(2,1)} %broadcast_select_fusion), calls=%async_computation.5 | async-start | bytes 524288 | tf_op jit(solution)/shard_map/all_to_all | solution.py:323
  147.7 4.0 %fusion.1 = bf16[1,2048,512]{2,1,0:T(8,128)(2,1)} fusion(bf16[384,2048]{1,0:T(8,128)(2,1)} %all-gather.5.cloned.1.call-done, bf16[384,512]{1,0:T(8,128)(2,1)S(1)} %get-tuple-element.50), kind=kOutput, calls=%fused_computation.5 | convolution fusion | flops 806354944 | bytes 4063232 | tf_op jit(solution)/shard_map/dot_general | solution.py:304
  151.7 8.5 %shard_map.200 = (f32[128,128]{1,0:T(8,128)}, f32[128,128]{1,0:T(8,128)}, f32[256,128]{1,0:T(8,128)}, f32[128,128]{1,0:T(8,128)}, f32[128,128]{1,0:T(8,128)}) custom-call(f32[256,128]{1,0:T(8,128)} %get-tuple-element.34.dm_ref, bf16[128,128]{1,0:T(8,128)(2,1)} %q_ref.7, bf16[128,128]{1,0:T(8,128)(2,1)} %k_ref.5, bf16[256,128]{1,0:T(8,128)(2,1)} %v_ref.5, ...), custom_call_target="tpu_custom_call" | custom-call | flops 2147483648 | bytes 1048576 | tf_op jit(solution)/shard_map/pallas_call | solution.py:196
  160.9 4.1 %shard_map.201 = (f32[128,128]{1,0:T(8,128)}, f32[256,128]{1,0:T(8,128)}, f32[128,128]{1,0:T(8,128)}) custom-call(s32[1]{0:T(128)} %bitcast.18.me_ref, bf16[8,128,128]{2,1,0:T(8,128)(2,1)} %copy-done.4, bf16[8,128,128]{2,1,0:T(8,128)(2,1)} %all_to_all.27.recv_ref.first_ref, f32[128,128]{1,0:T(8,128)} %get-tuple-element.36.carried_ref, ...), custom_call_target="tpu_custom_call" | custom-call | flops 268435456 | bytes 1048576 | tf_op jit(solution)/shard_map/pallas_call | solution.py:196
  165.0 30.6 %reduce-scatter.5.cloned.1.call-done = bf16[256,256]{1,0:T(8,128)(2,1)} async-done(((bf16[2048,256]{1,0:T(8,128)(2,1)}), bf16[256,256]{1,0:T(8,128)(2,1)}) %reduce-scatter.5.cloned.1.call-update) | async-done | bytes 131088 | tf_op jit(solution)/shard_map/reduce_scatter | solution.py:312
  195.6 1.6 convert_element_type.99
  (40 shorter events, 4.6 us)
Async XLA Ops:
  7.2 40.9 %copy-start = (bf16[1,2048,512]{2,1,0:T(8,128)(2,1)S(1)}, bf16[1,2048,512]{2,1,0:T(8,128)(2,1)}, u32[]{:S(2)}) copy-start(bf16[1,2048,512]{2,1,0:T(8,128)(2,1)} %param.25) | copy-start | bytes 6291460
  7.2 40.9 %all-gather.5.cloned.1.call-start = ((), (), s32[]{:S(2)}) async-start(), calls=%async_computation.8 | async-start | bytes 1966080 | tf_op jit(solution)/shard_map/all_gather | solution.py:260
  29.5 39.7 %all-gather.3.cloned.1.call-start = ((), (), s32[]{:S(2)}) async-start(), calls=%async_computation.7 | async-start | bytes 1966080 | tf_op jit(solution)/shard_map/all_gather | solution.py:260
  46.9 58.1 %reduce-scatter.3.cloned.1.call-start = ((), (), s32[]{:S(2)}) async-start(), calls=%async_computation.9 | async-start | bytes 1966080 | tf_op jit(solution)/shard_map/reduce_scatter | solution.py:299
  48.1 3.4 %copy-start.1 = (bf16[1,2048,512]{2,1,0:T(8,128)(2,1)S(1)}, bf16[1,2048,512]{2,1,0:T(8,128)(2,1)}, u32[]{:S(2)}) copy-start(bf16[1,2048,512]{2,1,0:T(8,128)(2,1)} %param.26) | copy-start | bytes 6291460
  48.1 3.4 %copy-start.7 = (bf16[384,2048]{1,0:T(8,128)(2,1)S(1)}, bf16[384,2048]{1,0:T(8,128)(2,1)}, u32[]{:S(2)}) copy-start(bf16[384,2048]{1,0:T(8,128)(2,1)} %all-gather.5.cloned.1.call-done) | copy-start | bytes 4718596
  72.9 1.6 copy-start.2
  74.5 2.2 %copy-start.6 = (f32[128]{0:T(128)S(1)}, f32[128]{0:T(128)}, u32[]{:S(2)}) copy-start(f32[128]{0:T(128)} %param.19) | copy-start | bytes 1540
  84.9 37.2 %copy-start.5 = (bf16[128,512]{1,0:T(8,128)(2,1)S(1)}, bf16[128,512]{1,0:T(8,128)(2,1)}, u32[]{:S(2)}) copy-start(bf16[128,512]{1,0:T(8,128)(2,1)} %param.24) | copy-start | bytes 393220
  105.0 17.1 %all-to-all-start.2 = ((bf16[8,48,512]{2,1,0:T(8,128)(2,1)}), bf16[8,48,512]{2,1,0:T(8,128)(2,1)S(1)}, u32[]{:S(2)}, u32[]{:S(2)}) async-start(bf16[8,48,512]{2,1,0:T(8,128)(2,1)} %bitcast.70), calls=%async_computation.3 | async-start | bytes 786432 | tf_op jit(solution)/shard_map/all_to_all | solution.py:305
  110.5 85.1 %reduce-scatter.5.cloned.1.call-start = ((), (), s32[]{:S(2)}) async-start(), calls=%async_computation.10 | async-start | bytes 1179648 | tf_op jit(solution)/shard_map/reduce_scatter | solution.py:312
  131.2 4.2 %copy-start.8 = (bf16[384,2048]{1,0:T(8,128)(2,1)S(1)}, bf16[384,2048]{1,0:T(8,128)(2,1)}, u32[]{:S(2)}) copy-start(bf16[384,2048]{1,0:T(8,128)(2,1)} %all-gather.3.cloned.1.call-done) | copy-start | bytes 4718596
  131.2 4.2 %copy-start.9 = (f32[384,512]{1,0:T(8,128)S(1)}, f32[384,512]{1,0:T(8,128)}, u32[]{:S(2)}) copy-start(f32[384,512]{1,0:T(8,128)} %fusion.5) | copy-start | bytes 2359300
  131.2 4.2 %copy-start.10 = (f32[384,512]{1,0:T(8,128)S(1)}, f32[384,512]{1,0:T(8,128)}, u32[]{:S(2)}) copy-start(f32[384,512]{1,0:T(8,128)} %fusion.8) | copy-start | bytes 2359300
  135.4 2.7 %copy-start.3 = (bf16[2048,256]{1,0:T(8,128)(2,1)S(1)}, bf16[2048,256]{1,0:T(8,128)(2,1)}, u32[]{:S(2)}) copy-start(bf16[2048,256]{1,0:T(8,128)(2,1)} %param.20) | copy-start | bytes 3145732
  144.0 16.2 %all-to-all-start.4 = ((bf16[8,128,128]{2,1,0:T(8,128)(2,1)}), bf16[8,128,128]{2,1,0:T(8,128)(2,1)S(1)}, u32[]{:S(2)}, u32[]{:S(2)}) async-start(bf16[8,128,128]{2,1,0:T(8,128)(2,1)} %broadcast_select_fusion), calls=%async_computation.5 | async-start | bytes 524288 | tf_op jit(solution)/shard_map/all_to_all | solution.py:323
  160.2 0.7 copy-start.4
Sparse Core Ops, SparseCore 0:
  29.6 18.3 all-gather.4
  49.6 19.6 all-gather.2
  76.9 28.0 reduce-scatter.2
  131.3 64.2 reduce-scatter.4

commit v2 on v1

--- a/solution.py
+++ b/solution.py
@@ -271,6 +271,12 @@
         [queries, input_key_matrix, input_value_matrix, decay_preactivation, extra_log_decay,
          speed], 1 << 28)
     peer = lax.broadcasted_iota(jnp.int32, (experts, 1, 1), 0)
+    gate_local = expert_gate_weight[0]
+    up_local = expert_up_weight[0]
+    gate_pre = jnp.dot(rows_x, gate_local, preferred_element_type=F32)
+    up_pre = jnp.dot(rows_x, up_local, preferred_element_type=F32)
+    rows_dy, fwd_sum, bwd_sum, gate_pre, up_pre = lax.optimization_barrier(
+        (rows_dy, fwd_sum, bwd_sum, gate_pre, up_pre))
     sums = lax.all_to_all(jnp.where(peer > index, fwd_sum[None], bwd_sum[None]),
                           "sp", split_axis=0, concat_axis=0, tiled=True)
     carried, normed, inv_rms, mix_rows = per_head(
@@ -278,12 +284,10 @@
         [((channels, 2 * VAL_DIM), F32), ((values, tok_rows), F32), ((heads * 8, tok_rows), F32),
          ((values, tok_rows), BF16)],
         [me, sums, queries, cum, inner], 1 << 26, scalars=1)
-
-    gate_local = expert_gate_weight[0]
-    up_local = expert_up_weight[0]
+    all_mix = lax.all_to_all(jnp.broadcast_to(mix_rows[None], (experts, values, tok_rows)),
+                             "sp", split_axis=0, concat_axis=0, tiled=True)
+
     down_local = expert_down_weight[0]
-    gate_pre = jnp.dot(rows_x, gate_local, preferred_element_type=F32)
-    up_pre = jnp.dot(rows_x, up_local, preferred_element_type=F32)
     gate_sig = jax.nn.sigmoid(gate_pre)
     gate_act = gate_pre * gate_sig
     hidden = (gate_act * up_pre).astype(BF16)
@@ -302,6 +306,7 @@
     grad_down = lax.dot_general(hidden, rows_dy, tn, preferred_element_type=F32).astype(BF16)
     grad_gate = lax.dot_general(rows_x, grad_gate_pre, tn, preferred_element_type=F32).astype(BF16)
     grad_up = lax.dot_general(rows_x, grad_up_pre, tn, preferred_element_type=F32).astype(BF16)
+    summed, all_mix = lax.optimization_barrier((summed, all_mix))
     returned = lax.all_to_all(summed, "sp", split_axis=0, concat_axis=0, tiled=True)
     picked = jnp.dot(place, returned.reshape(slots, part_width), preferred_element_type=F32)
     grad_rows = (cotangent.astype(F32) + picked).astype(BF16)
@@ -309,14 +314,6 @@
     grad_normed = lax.dot_general(
         output_weight_matrix, full_rows, (((0,), (1,)), ((), ())), preferred_element_type=F32
     )
-    grad_out_proj = lax.psum_scatter(
-        lax.dot_general(
-            full_rows, mix_rows, (((0,), (1,)), ((), ())), preferred_element_type=F32
-        ).astype(BF16),
-        "sp",
-        scatter_dimension=0,
-        tiled=True,
-    ).astype(F32)
     grad_mixed, fwd_source, bwd_source = per_head(
         source_kernel, heads, [((values, tok_rows), F32), state, state],
         [grad_normed, normed, inv_rms, queries, cum], 1 << 26)
@@ -328,6 +325,14 @@
         [by_channel, by_channel, ((values, tok_rows), F32), by_channel, by_channel],
         [grad_mixed, queries, input_key_matrix, input_value_matrix, cum, scores, carried],
         1 << 29)
+    full_rows, dk = lax.optimization_barrier((full_rows, dk))
+    rows_block = model_width // experts
+    all_rows = lax.all_to_all(full_rows.reshape(tok_rows, experts, rows_block).swapaxes(0, 1),
+                              "sp", split_axis=0, concat_axis=0, tiled=True)
+    grad_out_proj = lax.dot_general(
+        all_rows.reshape(experts * tok_rows, rows_block),
+        all_mix.swapaxes(1, 2).reshape(experts * tok_rows, values),
+        tn, preferred_element_type=F32)
     grad_keys, grad_values, grad_logit = per_head(
         last_kernel, heads, [by_channel, ((values, tok_rows), F32), by_channel],
         [me, sources, sums, carried, input_key_matrix, input_value_matrix, cum,

time: 205 us -> 186 us (0.907)
  waiting for transfers between devices: 59.9 us -> 21.7 us
  blocking collectives: 55.5 us -> 73.6 us
  starting transfers between devices: 9.36 us -> 13.4 us
  matrix products: 28.5 us -> 25.9 us
  other arithmetic: 5.99 us -> 3.55 us
    reduce_scatter x1 -> x0, waiting for transfers between devices: 30.6 us -> none  [body(): lax.psum_scatter(lax.dot_general(full_rows, mix_rows, (((0,), (1,)), ((),...]
    all_to_all x0 -> x1, blocking collectives: none -> 17.9 us  [body(): lax.all_to_all(jnp.broadcast_to(mix_rows[None], (experts, values, tok_row...]
    all_gather x2, waiting for transfers between devices: 17.1 us -> 9.48 us  [exchange(): lax.all_gather(rows.reshape(slots, part_width), 'tp', axis=1, tiled=True)]
    all_to_all x0 -> x1, starting transfers between devices: none -> 6 us  [body(): lax.all_to_all(full_rows.reshape(tok_rows, experts, rows_block).swapaxes(...]
    reduce_scatter x1, waiting for transfers between devices: 4.45 us -> 0.01 us  [body(): lax.psum_scatter(partial_value.astype(BF16), 'tp', scatter_dimension=1, t...]
    all_to_all x1, waiting for transfers between devices: 7.75 us -> 11.4 us  [body(): lax.all_to_all(summed, 'sp', split_axis=0, concat_axis=0, tiled=True)]
  transfers between devices with their start and end apart: 6 -> 6, of which waited for: 5 -> 3; matrix products, arithmetic and copies ran while one was open for 11% -> 10% of each run, Pallas kernels for 13% -> 13%
where the time goes in v2:
time: 186 us; the launch traced here: 185 us
  blocking collectives  73.6 us (40%)
  Pallas kernels  26.9 us (14%)
  matrix products  25.9 us (14%)
  waiting for transfers between devices  21.7 us (12%)
  between operations  14 us (8%)
  starting transfers between devices  13.4 us (7%)
  local copies, waits for them, and re-layouts  5.48 us (3%)
  other arithmetic  3.55 us (2%)
    all_to_all x2, blocking collectives, exchange(): rows = lax.all_to_all(rows, 'sp', split_axis=0, concat_axis=0, tiled=True)  34.3 us
    pallas_call x5, Pallas kernels, per_head(): pl.pallas_call(kernel, grid=(heads,), in_specs=in_specs, out_specs=[spec(...  26.9 us
    all_to_all x1, blocking collectives, body(): lax.all_to_all(jnp.broadcast_to(mix_rows[None], (experts, values, tok_row...  17.9 us
    all_to_all x1, blocking collectives, body(): lax.all_to_all(jnp.where(peer > index, fwd_sum[None], bwd_sum[None]), 'sp...  14.9 us
    all_to_all x1, waiting for transfers between devices, body(): lax.all_to_all(summed, 'sp', split_axis=0, concat_axis=0, tiled=True)  11.4 us
    all_gather x2, waiting for transfers between devices, exchange(): lax.all_gather(rows.reshape(slots, part_width), 'tp', axis=1, tiled=True)  9.48 us
    all_gather x1, blocking collectives, body(): full_rows = lax.all_gather(grad_rows, 'tp', axis=1, tiled=True)  6.5 us
    all_to_all x1, starting transfers between devices, body(): lax.all_to_all(full_rows.reshape(tok_rows, experts, rows_block).swapaxes(...  6 us
  transfers between devices with their start and end apart: 6, of which 3 were waited for; matrix products, arithmetic and copies ran while one was open for 10% of the time, Pallas kernels for 13%

profile of v2, /device:TPU:0, one launch (start us, length us, event | category | flops | bytes accessed | tf_op | source)
XLA Modules:
  0.0 184.5 jit_solution(9091092912472847958)
XLA Ops:
  7.2 0.8 slice_bitcast_fusion.3
  9.0 1.3 convolution_convert_fusion.3
  10.3 19.2 %all_to_all.35 = bf16[8,48,512]{2,1,0:T(8,128)(2,1)} all-to-all(bf16[8,48,512]{2,1,0:T(8,128)(2,1)S(1)} %bitcast.77), channel_id=1, replica_groups=mesh['sp'=8,'tp'=4] {'sp'}, dimensions={0} | all-to-all | bytes 786432 | tf_op jit(solution)/shard_map/all_to_all | solution.py:259
  30.5 1.0 fusion.15
  31.8 15.1 %all_to_all.36 = bf16[8,48,512]{2,1,0:T(8,128)(2,1)} all-to-all(bf16[8,48,512]{2,1,0:T(8,128)(2,1)S(1)} %bitcast.80), channel_id=1, replica_groups=mesh['sp'=8,'tp'=4] {'sp'}, dimensions={0} | all-to-all | bytes 786432 | tf_op jit(solution)/shard_map/all_to_all | solution.py:259
  47.7 7.4 %shard_map.197 = (bf16[512,128]{1,0:T(8,128)(2,1)}, f32[256,128]{1,0:T(8,128)}, f32[128,128]{1,0:T(8,128)}, bf16[128,128]{1,0:T(8,128)(2,1)}, bf16[128,128]{1,0:T(8,128)(2,1)}) custom-call(bf16[128,128]{1,0:T(8,128)(2,1)} %q_ref.7, bf16[128,128]{1,0:T(8,128)(2,1)} %k_ref.5, bf16[256,128]{1,0:T(8,128)(2,1)} %v_ref.5, bf16[128,128]{1,0:T(8,128)(2,1)} %pre_ref.3, ...), custom_call_target="tpu_custom_call" | custom-call | flops 1073741824 | bytes 1048576 | tf_op jit(solution)/shard_map/pallas_call | solution.py:196
  55.1 2.6 %fusion.10 = f32[384,512]{1,0:T(8,128)S(1)} fusion(bf16[384,2048]{1,0:T(8,128)(2,1)} %all-gather.5.cloned.1.call-done, bf16[1,2048,512]{2,1,0:T(8,128)(2,1)S(1)} %copy-done), kind=kOutput, calls=%fused_computation.14 | convolution fusion | flops 805306368 | bytes 4456448 | tf_op jit(solution)/shard_map/dot_general | solution.py:276
  58.0 1.9 %fusion.6 = f32[384,512]{1,0:T(8,128)} fusion(bf16[384,2048]{1,0:T(8,128)(2,1)S(1)} %copy-done.11, bf16[1,2048,512]{2,1,0:T(8,128)(2,1)S(1)} %copy-done.1), kind=kOutput, calls=%fused_computation.10 | convolution fusion | flops 805306368 | bytes 4456448 | tf_op jit(solution)/shard_map/dot_general | solution.py:277
  59.8 9.5 %all-gather.3.cloned.1.call-done = bf16[384,2048]{1,0:T(8,128)(2,1)} async-done(((bf16[384,512]{1,0:T(8,128)(2,1)}), bf16[384,2048]{1,0:T(8,128)(2,1)}) %all-gather.3.cloned.1.call-update) | async-done | bytes 1572880 | tf_op jit(solution)/shard_map/all_gather | solution.py:260
  69.3 3.4 %multiply_convert_fusion.1 = (bf16[384,512]{1,0:T(8,128)(2,1)S(1)}, bf16[384,512]{1,0:T(8,128)(2,1)S(1)}) fusion(f32[384,512]{1,0:T(8,128)S(1)} %fusion.10, f32[384,512]{1,0:T(8,128)} %fusion.6, bf16[384,2048]{1,0:T(8,128)(2,1)} %all-gather.3.cloned.1.call-done, bf16[1,512,2048]{2,1,0:T(8,128)(2,1)} %param.27), kind=kOutput, calls=%fused_computation.23 | convolution fusion | flops 807862272 | bytes 6029312 | tf_op jit(solution)/shard_map/dot_general | solution.py:294
  72.8 1.0 fusion.8
  73.8 0.8 copy-done.2
  74.7 2.2 %add_convert_fusion = bf16[384,2048]{1,0:T(8,128)(2,1)} fusion(f32[384,2048]{1,0:T(8,128)S(1)} %fusion.8, bf16[384,512]{1,0:T(8,128)(2,1)S(1)} %get-tuple-element.68, bf16[1,2048,512]{2,1,0:T(8,128)(2,1)S(1)} %copy-done.2), kind=kOutput, calls=%fused_computation | convolution fusion | flops 806879232 | bytes 7208960 | tf_op jit(solution)/shard_map/dot_general | solution.py:300
  77.0 14.9 %all_to_all.37.recv_ref.first_ref = bf16[8,128,128]{2,1,0:T(8,128)(2,1)} all-to-all(bf16[8,128,128]{2,1,0:T(8,128)(2,1)S(1)} %broadcast_select_fusion.1), channel_id=1, replica_groups=mesh['sp'=8,'tp'=4] {'sp'}, dimensions={0} | all-to-all | bytes 524288 | tf_op jit(solution)/shard_map/all_to_all | solution.py:280
  91.8 3.7 %shard_map.198 = (f32[128,128]{1,0:T(8,128)}, f32[256,128]{1,0:T(8,128)}, f32[32,128]{1,0:T(8,128)}, bf16[256,128]{1,0:T(8,128)(2,1)}) custom-call(s32[1]{0:T(128)} %bitcast.17.me_ref, bf16[8,128,128]{2,1,0:T(8,128)(2,1)} %all_to_all.37.recv_ref.first_ref, bf16[128,128]{1,0:T(8,128)(2,1)} %q_ref.7, f32[128,128]{1,0:T(8,128)} %get-tuple-element.44.cum_ref, ...), custom_call_target="tpu_custom_call" | custom-call | flops 268435456 | bytes 1048576 | tf_op jit(solution)/shard_map/pallas_call | solution.py:196
  95.6 0.9 copy.23
  96.5 17.9 %all_to_all.38 = bf16[8,256,128]{1,2,0:T(8,128)(2,1)S(1)} all-to-all(bf16[8,256,128]{1,2,0:T(8,128)(2,1)S(1)} %broadcast_in_dim.73), channel_id=1, replica_groups=mesh['sp'=8,'tp'=4] {'sp'}, dimensions={0} | all-to-all | bytes 1048576 | tf_op jit(solution)/shard_map/all_to_all | solution.py:287
  114.4 3.6 %all-to-all-start.4 = ((bf16[8,48,512]{2,1,0:T(8,128)(2,1)}), bf16[8,48,512]{2,1,0:T(8,128)(2,1)S(1)}, u32[]{:S(2)}, u32[]{:S(2)}) async-start(bf16[8,48,512]{2,1,0:T(8,128)(2,1)} %bitcast.78), calls=%async_computation.5 | async-start | bytes 786432 | tf_op jit(solution)/shard_map/all_to_all | solution.py:310
  118.0 11.4 %all-to-all-done.4 = bf16[8,48,512]{2,1,0:T(8,128)(2,1)S(1)} async-done(((bf16[8,48,512]{2,1,0:T(8,128)(2,1)}), bf16[8,48,512]{2,1,0:T(8,128)(2,1)S(1)}, u32[]{:S(2)}, u32[]{:S(2)}) %all-to-all-start.4) | async-done | bytes 393248 | tf_op jit(solution)/shard_map/all_to_all | solution.py:310
  129.7 6.5 %all_gather.11 = bf16[128,2048]{1,0:T(8,128)(2,1)S(1)} all-gather(bf16[128,512]{1,0:T(8,128)(2,1)S(1)} %fusion.12), channel_id=1, replica_groups=mesh['sp'=8,'tp'=4] {'tp'}, dimensions={1}, use_global_device_ids=true | all-gather | bytes 655360 | tf_op jit(solution)/shard_map/all_gather | solution.py:313
  136.2 2.4 %convolution_bitcast_fusion.1.gn_ref = f32[256,128]{1,0:T(8,128)} fusion(bf16[128,2048]{1,0:T(8,128)(2,1)S(1)} %all_gather.11, bf16[2048,256]{1,0:T(8,128)(2,1)} %param.20), kind=kOutput, calls=%fused_computation.21 | convolution fusion | flops 134217728 | bytes 1703936 | tf_op jit(solution)/shard_map/dot_general | solution.py:314
  138.6 3.2 %shard_map.199 = (f32[256,128]{1,0:T(8,128)}, bf16[128,128]{1,0:T(8,128)(2,1)}, bf16[128,128]{1,0:T(8,128)(2,1)}) custom-call(f32[256,128]{1,0:T(8,128)} %convolution_bitcast_fusion.1.gn_ref, f32[256,128]{1,0:T(8,128)} %get-tuple-element.48.normed_ref, f32[32,128]{1,0:T(8,128)} %get-tuple-element.49.inv_ref, bf16[128,128]{1,0:T(8,128)(2,1)} %q_ref.7, ...), custom_call_target="tpu_custom_call" | custom-call | flops 268435456 | bytes 1048576 | tf_op jit(solution)/shard_map/pallas_call | solution.py:196
  141.8 1.6 broadcast_select_fusion
  143.3 3.7 %all-to-all-start.5 = ((bf16[8,128,128]{2,1,0:T(8,128)(2,1)}), bf16[8,128,128]{2,1,0:T(8,128)(2,1)S(1)}, u32[]{:S(2)}, u32[]{:S(2)}) async-start(bf16[8,128,128]{2,1,0:T(8,128)(2,1)} %broadcast_select_fusion), calls=%async_computation.6 | async-start | bytes 524288 | tf_op jit(solution)/shard_map/all_to_all | solution.py:320
  147.0 8.5 %shard_map.200 = (f32[128,128]{1,0:T(8,128)}, f32[128,128]{1,0:T(8,128)}, f32[256,128]{1,0:T(8,128)}, f32[128,128]{1,0:T(8,128)}, f32[128,128]{1,0:T(8,128)}) custom-call(f32[256,128]{1,0:T(8,128)} %get-tuple-element.50.dm_ref, bf16[128,128]{1,0:T(8,128)(2,1)} %q_ref.7, bf16[128,128]{1,0:T(8,128)(2,1)} %k_ref.5, bf16[256,128]{1,0:T(8,128)(2,1)} %v_ref.5, ...), custom_call_target="tpu_custom_call" | custom-call | flops 2147483648 | bytes 1048576 | tf_op jit(solution)/shard_map/pallas_call | solution.py:196
  155.5 1.0 copy.28
  156.5 6.0 %all-to-all-start.6 = ((bf16[8,128,256]{1,2,0:T(8,128)(2,1)}), bf16[8,128,256]{1,2,0:T(8,128)(2,1)S(1)}, u32[]{:S(2)}, u32[]{:S(2)}) async-start(bf16[8,128,256]{1,2,0:T(8,128)(2,1)} %bitcast.74), calls=%async_computation.7 | async-start | bytes 1048576 | tf_op jit(solution)/shard_map/all_to_all | solution.py:330
  162.6 4.2 %fusion = bf16[1,2048,512]{2,1,0:T(8,128)(2,1)} fusion(bf16[384,2048]{1,0:T(8,128)(2,1)} %all-gather.5.cloned.1.call-done, bf16[384,512]{1,0:T(8,128)(2,1)} %copy-done.6), kind=kOutput, calls=%fused_computation.4 | convolution fusion | flops 806354944 | bytes 4063232 | tf_op jit(solution)/shard_map/dot_general | solution.py:307
  166.8 2.6 %fusion.1 = bf16[1,2048,512]{2,1,0:T(8,128)(2,1)} fusion(bf16[384,2048]{1,0:T(8,128)(2,1)S(1)} %copy-done.12, bf16[384,512]{1,0:T(8,128)(2,1)S(1)} %copy-done.5), kind=kOutput, calls=%fused_computation.5 | convolution fusion | flops 806354944 | bytes 4063232 | tf_op jit(solution)/shard_map/dot_general | solution.py:308
  169.4 2.7 %fusion.2 = bf16[1,512,2048]{2,1,0:T(8,128)(2,1)} fusion(bf16[384,2048]{1,0:T(8,128)(2,1)S(1)} %copy-done.13, f32[384,512]{1,0:T(8,128)S(1)} %copy-done.16, f32[384,512]{1,0:T(8,128)S(1)} %copy-done.15), kind=kOutput, calls=%fused_computation.6 | convolution fusion | flops 807534592 | bytes 5242880 | tf_op jit(solution)/shard_map/dot_general | solution.py:306
  172.1 4.1 %shard_map.201 = (f32[128,128]{1,0:T(8,128)}, f32[256,128]{1,0:T(8,128)}, f32[128,128]{1,0:T(8,128)}) custom-call(s32[1]{0:T(128)} %bitcast.17.me_ref, bf16[8,128,128]{2,1,0:T(8,128)(2,1)} %copy-done.3, bf16[8,128,128]{2,1,0:T(8,128)(2,1)} %all_to_all.37.recv_ref.first_ref, f32[128,128]{1,0:T(8,128)} %get-tuple-element.52.carried_ref, ...), custom_call_target="tpu_custom_call" | custom-call | flops 268435456 | bytes 1048576 | tf_op jit(solution)/shard_map/pallas_call | solution.py:196
  177.0 1.0 convolution_bitcast_fusion
  (54 shorter events, 4.5 us)
Async XLA Ops:
  7.2 47.9 %copy-start = (bf16[1,2048,512]{2,1,0:T(8,128)(2,1)S(1)}, bf16[1,2048,512]{2,1,0:T(8,128)(2,1)}, u32[]{:S(2)}) copy-start(bf16[1,2048,512]{2,1,0:T(8,128)(2,1)} %param.25) | copy-start | bytes 6291460
  7.2 47.9 %all-gather.5.cloned.1.call-start = ((), (), s32[]{:S(2)}) async-start(), calls=%async_computation.9 | async-start | bytes 1966080 | tf_op jit(solution)/shard_map/all_gather | solution.py:260
  10.3 36.7 %copy-start.10 = (f32[128]{0:T(128)S(1)}, f32[128]{0:T(128)}, u32[]{:S(2)}) copy-start(f32[128]{0:T(128)} %param.19) | copy-start | bytes 1540
  29.5 39.8 %all-gather.3.cloned.1.call-start = ((), (), s32[]{:S(2)}) async-start(), calls=%async_computation.8 | async-start | bytes 1966080 | tf_op jit(solution)/shard_map/all_gather | solution.py:260
  46.9 67.5 %reduce-scatter.2.cloned.1.call-start = ((), (), s32[]{:S(2)}) async-start(), calls=%async_computation.10 | async-start | bytes 1966080 | tf_op jit(solution)/shard_map/reduce_scatter | solution.py:303
  55.1 2.6 %copy-start.1 = (bf16[1,2048,512]{2,1,0:T(8,128)(2,1)S(1)}, bf16[1,2048,512]{2,1,0:T(8,128)(2,1)}, u32[]{:S(2)}) copy-start(bf16[1,2048,512]{2,1,0:T(8,128)(2,1)} %param.26) | copy-start | bytes 6291460
  55.1 2.9 %copy-start.11 = (bf16[384,2048]{1,0:T(8,128)(2,1)S(1)}, bf16[384,2048]{1,0:T(8,128)(2,1)}, u32[]{:S(2)}) copy-start(bf16[384,2048]{1,0:T(8,128)(2,1)} %all-gather.5.cloned.1.call-done) | copy-start | bytes 4718596
  58.0 11.3 %copy-start.14 = (f32[384,512]{1,0:T(8,128)}, f32[384,512]{1,0:T(8,128)S(1)}, u32[]{:S(2)}) copy-start(f32[384,512]{1,0:T(8,128)S(1)} %fusion.10) | copy-start | bytes 2359300
  72.8 1.0 copy-start.6
  72.8 1.0 copy-start.4
  72.8 1.9 %copy-start.2 = (bf16[1,2048,512]{2,1,0:T(8,128)(2,1)S(1)}, bf16[1,2048,512]{2,1,0:T(8,128)(2,1)}, u32[]{:S(2)}) copy-start(bf16[1,2048,512]{2,1,0:T(8,128)(2,1)} %param.26) | copy-start | bytes 6291460
  74.7 2.2 %copy-start.8 = (bf16[128,128]{1,0:T(8,128)(2,1)S(1)}, bf16[128,128]{1,0:T(8,128)(2,1)}, u32[]{:S(2)}) copy-start(bf16[128,128]{1,0:T(8,128)(2,1)} %get-tuple-element.42) | copy-start | bytes 98308
  74.7 2.2 %copy-start.9 = (bf16[128,128]{1,0:T(8,128)(2,1)S(1)}, bf16[128,128]{1,0:T(8,128)(2,1)}, u32[]{:S(2)}) copy-start(bf16[128,128]{1,0:T(8,128)(2,1)} %get-tuple-element.43) | copy-start | bytes 98308
  77.0 52.4 %copy-start.7 = (bf16[128,512]{1,0:T(8,128)(2,1)S(1)}, bf16[128,512]{1,0:T(8,128)(2,1)}, u32[]{:S(2)}) copy-start(bf16[128,512]{1,0:T(8,128)(2,1)} %param.24) | copy-start | bytes 393220
  114.4 15.0 %all-to-all-start.4 = ((bf16[8,48,512]{2,1,0:T(8,128)(2,1)}), bf16[8,48,512]{2,1,0:T(8,128)(2,1)S(1)}, u32[]{:S(2)}, u32[]{:S(2)}) async-start(bf16[8,48,512]{2,1,0:T(8,128)(2,1)} %bitcast.78), calls=%async_computation.5 | async-start | bytes 786432 | tf_op jit(solution)/shard_map/all_to_all | solution.py:310
  143.3 13.2 %all-to-all-start.5 = ((bf16[8,128,128]{2,1,0:T(8,128)(2,1)}), bf16[8,128,128]{2,1,0:T(8,128)(2,1)S(1)}, u32[]{:S(2)}, u32[]{:S(2)}) async-start(bf16[8,128,128]{2,1,0:T(8,128)(2,1)} %broadcast_select_fusion), calls=%async_computation.6 | async-start | bytes 524288 | tf_op jit(solution)/shard_map/all_to_all | solution.py:320
  156.5 10.2 %copy-start.3 = (bf16[8,128,128]{2,1,0:T(8,128)(2,1)}, bf16[8,128,128]{2,1,0:T(8,128)(2,1)S(1)}, u32[]{:S(2)}) copy-start(bf16[8,128,128]{2,1,0:T(8,128)(2,1)S(1)} %all-to-all-done.5.recv_ref) | copy-start | bytes 786436
  156.5 20.4 %all-to-all-start.6 = ((bf16[8,128,256]{1,2,0:T(8,128)(2,1)}), bf16[8,128,256]{1,2,0:T(8,128)(2,1)S(1)}, u32[]{:S(2)}, u32[]{:S(2)}) async-start(bf16[8,128,256]{1,2,0:T(8,128)(2,1)} %bitcast.74), calls=%async_computation.7 | async-start | bytes 1048576 | tf_op jit(solution)/shard_map/all_to_all | solution.py:330
  162.5 4.2 %copy-start.5 = (bf16[384,512]{1,0:T(8,128)(2,1)S(1)}, bf16[384,512]{1,0:T(8,128)(2,1)}, u32[]{:S(2)}) copy-start(bf16[384,512]{1,0:T(8,128)(2,1)} %copy-done.4) | copy-start | bytes 1179652
  162.6 4.2 %copy-start.12 = (bf16[384,2048]{1,0:T(8,128)(2,1)S(1)}, bf16[384,2048]{1,0:T(8,128)(2,1)}, u32[]{:S(2)}) copy-start(bf16[384,2048]{1,0:T(8,128)(2,1)} %all-gather.5.cloned.1.call-done) | copy-start | bytes 4718596
  166.8 2.6 %copy-start.13 = (bf16[384,2048]{1,0:T(8,128)(2,1)S(1)}, bf16[384,2048]{1,0:T(8,128)(2,1)}, u32[]{:S(2)}) copy-start(bf16[384,2048]{1,0:T(8,128)(2,1)} %all-gather.3.cloned.1.call-done) | copy-start | bytes 4718596
  166.8 2.6 %copy-start.15 = (f32[384,512]{1,0:T(8,128)S(1)}, f32[384,512]{1,0:T(8,128)}, u32[]{:S(2)}) copy-start(f32[384,512]{1,0:T(8,128)} %copy-done.14) | copy-start | bytes 2359300
  166.8 2.6 %copy-start.16 = (f32[384,512]{1,0:T(8,128)S(1)}, f32[384,512]{1,0:T(8,128)}, u32[]{:S(2)}) copy-start(f32[384,512]{1,0:T(8,128)} %fusion.6) | copy-start | bytes 2359300
Sparse Core Ops, SparseCore 0:
  29.7 18.3 all-gather.4
  49.6 19.6 all-gather.2
  77.0 27.9 reduce-scatter.1
